TPU v7x, 32 devices: a whole 2x2x4 slice. The times are simulated.
32 devices in a mesh: tp: 8 (over z, y), dp: 4 (over x, core).
Axes of the slice: x: 2, y: 2, z: 4, core: 2. Of those that a mesh axis runs over, the one named last changes fastest.
Arguments:
- tokens: bfloat16 [96, 1024], P('tp', 'dp'), may hold values from -6 to 6
- lengths: int32 [96], P('dp'), may hold values from 1 to 8, 192 in all
- norm_gain: float32 [2, 1024], P(None, 'dp'), may hold values from 0.1 to 1.9
- w_gate: bfloat16 [2, 1024, 512], P(None, 'dp', 'tp'), may hold values from -0.1875 to 0.1875
- w_value: bfloat16 [2, 1024, 512], P(None, 'dp', 'tp'), may hold values from -0.1875 to 0.1875
- w_write: bfloat16 [2, 1024, 256], P(None, 'dp', 'tp'), may hold values from -0.1875 to 0.1875
- w_read: bfloat16 [2, 1024, 256], P(None, 'dp', 'tp'), may hold values from -0.1875 to 0.1875
- w_step: bfloat16 [2, 1024, 8], P(None, 'dp', 'tp'), may hold values from -0.1875 to 0.1875
- step_bias: float32 [2, 8], P(None, 'tp'), may hold values from -1 to 1
- decay_rate: float32 [2, 8], P(None, 'tp'), may hold values from 0.5 to 4
- skip_gain: float32 [2, 8], P(None, 'tp'), may hold values from 0.5 to 2
- conv_value_w: float32 [2, 4, 512], P(None, None, 'tp'), may hold values from -3 to 3
- conv_write_w: float32 [2, 4, 256], P(None, None, 'tp'), may hold values from -3 to 3
- conv_read_w: float32 [2, 4, 256], P(None, None, 'tp'), may hold values from -3 to 3
- group_gain: float32 [2, 512], P(None, 'tp'), may hold values from 0.1 to 1.9
- w_out: bfloat16 [2, 512, 1024], P(None, 'tp', 'dp'), may hold values from -0.25 to 0.25
- state: float32 [2, 96, 8, 64, 128], P(None, 'dp', 'tp'), may hold values from -0.6 to 0.6
- hist_value: bfloat16 [2, 96, 3, 512], P(None, 'dp', None, 'tp'), may hold values from -6 to 6
- hist_write: bfloat16 [2, 96, 3, 256], P(None, 'dp', None, 'tp'), may hold values from -6 to 6
- hist_read: bfloat16 [2, 96, 3, 256], P(None, 'dp', None, 'tp'), may hold values from -6 to 6
Outputs:
- mixed: float32 [96, 1024], P('tp', 'dp')
- new_state: float32 [2, 96, 8, 64, 128], P(None, 'dp', 'tp')
- new_hist_value: bfloat16 [2, 96, 3, 512], P(None, 'dp', None, 'tp')
- new_hist_write: bfloat16 [2, 96, 3, 256], P(None, 'dp', None, 'tp')
- new_hist_read: bfloat16 [2, 96, 3, 256], P(None, 'dp', None, 'tp')
Inputs may be any that keep to these rules, and one draw needn't show every extreme that they name: `lengths`: each sequence holds between 1 and 8 tokens before this step, and some sequence holds exactly 8.
All inputs are finite; a program needn't handle non-finite values.
Results may differ from a plain program's by a relative error of at most 0.03.
Values may be sent and summed in bfloat16 or wider, within the bound.
A program may use at most 64 MiB of HBM per device.

v0:
```python
import jax
import jax.numpy as jnp
from jax import lax
from jax.sharding import PartitionSpec as P

D = 1024
GROUPS = 2


norm_eps = 1e-05


def conv_update(history, current, conv_taps, live_mask):
    kept_hist = history.astype(jnp.float32) * live_mask[:, :, None]
    mixed_sum = (
        jnp.sum(kept_hist * conv_taps[None, :-1, :], axis=1)
        + current.astype(jnp.float32) * conv_taps[-1][None, :]
    )
    fresh_hist = jnp.concatenate(
        [kept_hist[:, 1:].astype(jnp.bfloat16), current[:, None, :]], axis=1
    )
    return (jax.nn.silu(mixed_sum), fresh_hist)


def body(
    tokens,
    lengths,
    norm_gain,
    w_gate,
    w_value,
    w_write,
    w_read,
    w_step,
    step_bias,
    decay_rate,
    skip_gain,
    conv_value_w,
    conv_write_w,
    conv_read_w,
    group_gain,
    w_out,
    state,
    hist_value,
    hist_write,
    hist_read,
):
    seq_here = state.shape[1]
    local_heads = state.shape[2]
    head_dim = state.shape[3]
    hist_len = hist_value.shape[2]
    all_heads = local_heads * lax.axis_size("tp")
    per_group = all_heads // GROUPS
    group_width = all_heads * head_dim // GROUPS
    heads_here = lax.axis_index("tp") * local_heads + jnp.arange(local_heads, dtype=jnp.int32)
    group_here = heads_here // per_group
    member = (group_here[:, None] == jnp.arange(GROUPS, dtype=jnp.int32)[None, :]).astype(
        jnp.float32
    )
    offsets = hist_len - jnp.arange(hist_len, dtype=jnp.int32)
    live_mask = (offsets[None, :] <= lengths[:, None]).astype(jnp.float32)
    gate_cols = w_gate.shape[2]
    value_cols = w_value.shape[2]
    write_cols = w_write.shape[2]
    read_cols = w_read.shape[2]
    gathered = lax.all_gather(tokens, "tp", axis=0, tiled=True).astype(jnp.float32)
    current = tokens
    states_out, values_out, writes_out, reads_out = ([], [], [], [])
    for layer_idx in range(2):
        row_squares = jnp.sum(gathered * gathered, axis=1)
        weights = jnp.concatenate(
            [
                w_gate[layer_idx],
                w_value[layer_idx],
                w_write[layer_idx],
                w_read[layer_idx],
                w_step[layer_idx],
            ],
            axis=1,
        )
        total_sq = lax.psum(row_squares, "dp")
        row_scale = lax.rsqrt(total_sq / D + norm_eps)
        normed = (gathered * row_scale[:, None] * norm_gain[layer_idx][None, :]).astype(
            jnp.bfloat16
        )

        def project():
            row_block = lax.slice_in_dim(normed, 0, seq_here * lax.axis_size("dp"), axis=0)
            return jnp.dot(row_block, weights, preferred_element_type=jnp.float32)

        mixed_in = lax.psum_scatter(project(), "dp", scatter_dimension=0, tiled=True)
        edge_one = gate_cols
        edge_two = edge_one + value_cols
        edge_three = edge_two + write_cols
        edge_four = edge_three + read_cols
        gate_part = mixed_in[:, :edge_one].astype(jnp.bfloat16)
        value_part = mixed_in[:, edge_one:edge_two].astype(jnp.bfloat16)
        write_part = mixed_in[:, edge_two:edge_three].astype(jnp.bfloat16)
        read_part = mixed_in[:, edge_three:edge_four].astype(jnp.bfloat16)
        step_raw = mixed_in[:, edge_four:]
        value_act, value_hist = conv_update(
            hist_value[layer_idx], value_part, conv_value_w[layer_idx], live_mask
        )
        write_act, write_hist = conv_update(
            hist_write[layer_idx], write_part, conv_write_w[layer_idx], live_mask
        )
        read_act, read_hist = conv_update(
            hist_read[layer_idx], read_part, conv_read_w[layer_idx], live_mask
        )
        write_all, read_all = (
            lax.all_gather(write_act, "tp", axis=1, tiled=True),
            lax.all_gather(read_act, "tp", axis=1, tiled=True),
        )
        write_heads = jnp.moveaxis(
            jnp.take(write_all.reshape(seq_here, -1, GROUPS), group_here, axis=2), 2, 1
        )
        read_heads = jnp.moveaxis(
            jnp.take(read_all.reshape(seq_here, -1, GROUPS), group_here, axis=2), 2, 1
        )
        step_size = jax.nn.softplus(step_raw + step_bias[layer_idx][None, :])
        decay_keep = jnp.exp(-decay_rate[layer_idx][None, :] * step_size)
        inputs = value_act.reshape(seq_here, local_heads, head_dim)
        updated = (
            decay_keep[:, :, None, None] * state[layer_idx]
            + (step_size[:, :, None] * inputs)[:, :, :, None] * write_heads[:, :, None, :]
        )
        readout = (
            jnp.einsum("shpn,shn->shp", updated, read_heads, precision=lax.Precision.HIGHEST)
            + skip_gain[layer_idx][None, :, None] * inputs
        )
        gated_out = readout * jax.nn.silu(gate_part.astype(jnp.float32)).reshape(
            seq_here, local_heads, head_dim
        )
        head_squares = jnp.sum(gated_out * gated_out, axis=2)
        group_squares = jnp.dot(head_squares, member, precision=lax.Precision.HIGHEST)
        group_total = lax.psum(group_squares, "tp")
        group_scale = lax.rsqrt(group_total / group_width + norm_eps)
        head_scale = jnp.take(group_scale, group_here, axis=1)
        scaled_out = (gated_out * head_scale[:, :, None]).reshape(seq_here, -1)
        mixer_out = (scaled_out * group_gain[layer_idx][None, :]).astype(jnp.bfloat16)
        proj_out = w_out[layer_idx]

        def emit_rows(shard_rows):
            return jnp.dot(shard_rows, proj_out, preferred_element_type=jnp.float32)

        partial_value = emit_rows(lax.all_gather(mixer_out, "dp", axis=0, tiled=True))
        if layer_idx == 0:
            rounded = lax.optimization_barrier(lax.psum(partial_value, "tp").astype(jnp.bfloat16))
            gathered = rounded.astype(jnp.float32)
        else:
            current = lax.psum_scatter(partial_value, "tp", scatter_dimension=0, tiled=True)
        states_out.append(updated)
        values_out.append(value_hist)
        writes_out.append(write_hist)
        reads_out.append(read_hist)
    return (
        current,
        jnp.stack(states_out),
        jnp.stack(values_out),
        jnp.stack(writes_out),
        jnp.stack(reads_out),
    )


def solution(mesh):
    in_specs = (
        P("tp", "dp"),
        P("dp"),
        P(None, "dp"),
        P(None, "dp", "tp"),
        P(None, "dp", "tp"),
        P(None, "dp", "tp"),
        P(None, "dp", "tp"),
        P(None, "dp", "tp"),
        P(None, "tp"),
        P(None, "tp"),
        P(None, "tp"),
        P(None, None, "tp"),
        P(None, None, "tp"),
        P(None, None, "tp"),
        P(None, "tp"),
        P(None, "tp", "dp"),
        P(None, "dp", "tp", None, None),
        P(None, "dp", None, "tp"),
        P(None, "dp", None, "tp"),
        P(None, "dp", None, "tp"),
    )
    out_specs = (
        P("tp", "dp"),
        P(None, "dp", "tp", None, None),
        P(None, "dp", None, "tp"),
        P(None, "dp", None, "tp"),
        P(None, "dp", None, "tp"),
    )
    return jax.shard_map(body, mesh=mesh, in_specs=in_specs, out_specs=out_specs, check_vma=False)
```

profile of v0, /device:TPU:0, one launch (start us, length us, event | category | flops | bytes accessed | tf_op | source)
XLA Modules:
  0.0 350.4 jit_solution(7639507683110838594)
XLA Ops:
  7.2 0.8 bitcast_dynamic-update-slice_fusion.3
  8.0 32.5 %all-gather = bf16[8,12,256]{2,1,0:T(8,128)(2,1)S(1)} all-gather(bf16[1,12,256]{2,1,0:T(8,128)(2,1)} %bitcast.206), channel_id=1, replica_groups=mesh['tp'=8,'dp'=4] {'tp'}, dimensions={0}, use_global_device_ids=true | all-gather | bytes 55296 | tf_op jit(solution)/shard_map/all_gather | solution.py:65
  40.5 0.8 fusion.47
  41.3 0.1 multiply_reduce_fusion
  41.4 5.7 %psum.35 = f32[96]{0:T(128)S(1)} all-reduce(f32[96]{0:T(128)S(1)} %multiply_reduce_fusion), channel_id=1, replica_groups=mesh['tp'=8,'dp'=4] {'dp'}, use_global_device_ids=true, to_apply=%region_1.2 | all-reduce | flops 96 | bytes 768 | tf_op jit(solution)/shard_map/psum | solution.py:80
  47.1 0.8 bitcast_dynamic-update-slice_fusion.2
  47.9 0.9 constant_dynamic-update-slice_fusion.2
  48.7 0.7 constant_dynamic-update-slice_fusion.1
  49.5 0.8 constant_dynamic-update-slice_fusion
  50.2 0.8 fusion.20
  51.2 0.7 slice_bitcast_fusion.10
  51.9 0.7 slice_bitcast_fusion.14
  52.6 0.7 slice_bitcast_fusion.9
  53.3 0.7 slice_bitcast_fusion.13
  54.0 0.7 slice_bitcast_fusion.11
  54.7 0.7 slice_bitcast_fusion.15
  55.4 1.3 fusion.50
  56.7 1.3 fusion.49
  58.0 1.3 fusion.48
  59.3 0.8 slice_bitcast_fusion.12
  60.1 0.7 compare_convert_fusion.1
  60.8 0.8 convert_multiply_fusion.7
  61.6 0.8 multiply_reduce_fusion.3
  62.5 0.9 convert_multiply_fusion.5
  64.7 0.6 dynamic-slice.22
  66.0 6.0 %reduce-scatter.5.cloned.1.call-done = f32[24,193]{1,0:T(8,128)} async-done(((f32[96,193]{1,0:T(8,128)}), f32[24,193]{1,0:T(8,128)}) %reduce-scatter.5.cloned.1.call-update) | async-done | bytes 18544 | tf_op jit(solution)/shard_map/reduce_scatter | solution.py:90
  72.0 0.8 convert.40
  73.1 30.5 %all-gather.2 = f32[8,32,24]{1,2,0:T(8,128)S(1)} all-gather(f32[1,32,24]{1,2,0:T(8,128)S(1)} %get-tuple-element.68), channel_id=1, replica_groups=mesh['tp'=8,'dp'=4] {'tp'}, dimensions={0}, use_global_device_ids=true | all-gather | bytes 27648 | tf_op jit(solution)/shard_map/all_gather | solution.py:111
  103.7 0.1 copy.43
  104.0 30.5 %all-gather.1 = f32[8,32,24]{1,2,0:T(8,128)S(1)} all-gather(f32[1,32,24]{1,2,0:T(8,128)S(1)} %get-tuple-element.67), channel_id=1, replica_groups=mesh['tp'=8,'dp'=4] {'tp'}, dimensions={0}, use_global_device_ids=true | all-gather | bytes 27648 | tf_op jit(solution)/shard_map/all_gather | solution.py:110
  134.5 0.1 copy.40
  134.8 0.8 exponential_reduce_fusion.1
  135.7 1.4 fusion.5
  137.2 0.8 multiply_reduce_fusion.8
  138.1 21.3 %psum.36 = f32[24,2]{0,1:T(2,128)S(1)} all-reduce(f32[24,2]{0,1:T(2,128)S(1)} %broadcast_multiply_fusion.3), channel_id=1, replica_groups=mesh['tp'=8,'dp'=4] {'tp'}, use_global_device_ids=true, to_apply=%region_7.9 | all-reduce | flops 48 | bytes 384 | tf_op jit(solution)/shard_map/psum | solution.py:135
  159.4 5.2 %all_gather.24 = bf16[96,64]{1,0:T(8,128)(2,1)S(1)} all-gather(bf16[24,64]{1,0:T(8,128)(2,1)S(1)} %multiply_convert_fusion.3), channel_id=1, replica_groups=mesh['tp'=8,'dp'=4] {'dp'}, dimensions={0}, use_global_device_ids=true | all-gather | bytes 15360 | tf_op jit(solution)/shard_map/all_gather | solution.py:145
  164.6 0.1 fusion.29
  164.7 33.8 %psum.37 = bf16[96,256]{1,0:T(8,128)(2,1)S(1)} all-reduce(f32[96,256]{1,0:T(8,128)S(1)} %fusion.29), channel_id=1, replica_groups=mesh['tp'=8,'dp'=4] {'tp'}, use_global_device_ids=true, to_apply=%region_8.11 | all-reduce | flops 24576 | bytes 147456 | tf_op jit(solution)/shard_map/psum | solution.py:147
  198.5 0.1 fusion.17
  198.6 6.0 %psum.38 = f32[96]{0:T(128)S(1)} all-reduce(f32[96]{0:T(128)S(1)} %fusion.17), channel_id=1, replica_groups=mesh['tp'=8,'dp'=4] {'dp'}, use_global_device_ids=true, to_apply=%region_10.13 | all-reduce | flops 96 | bytes 768 | tf_op jit(solution)/shard_map/psum | solution.py:80
  204.6 0.8 fusion.21
  205.5 17.6 %reduce-scatter.7.cloned.1.call-done = f32[24,193]{1,0:T(8,128)} async-done(((f32[96,193]{1,0:T(8,128)}), f32[24,193]{1,0:T(8,128)}) %reduce-scatter.7.cloned.1.call-update) | async-done | bytes 18544 | tf_op jit(solution)/shard_map/reduce_scatter | solution.py:90
  223.1 0.8 convert.42
  224.0 30.5 %all-gather.4 = f32[8,32,24]{1,2,0:T(8,128)S(1)} all-gather(f32[1,32,24]{1,2,0:T(8,128)S(1)} %get-tuple-element.66), channel_id=1, replica_groups=mesh['tp'=8,'dp'=4] {'tp'}, dimensions={0}, use_global_device_ids=true | all-gather | bytes 27648 | tf_op jit(solution)/shard_map/all_gather | solution.py:111
  254.6 0.1 copy.49
  254.7 30.5 %all-gather.3 = f32[8,32,24]{1,2,0:T(8,128)S(1)} all-gather(f32[1,32,24]{1,2,0:T(8,128)S(1)} %get-tuple-element.65), channel_id=1, replica_groups=mesh['tp'=8,'dp'=4] {'tp'}, dimensions={0}, use_global_device_ids=true | all-gather | bytes 27648 | tf_op jit(solution)/shard_map/all_gather | solution.py:110
  285.3 0.1 copy.46
  285.4 0.1 broadcast_select_fusion
  285.7 0.9 exponential_reduce_fusion
  286.7 1.4 fusion.2
  288.1 0.8 multiply_reduce_fusion.7
  289.0 21.3 %psum.39 = f32[24,2]{0,1:T(2,128)S(1)} all-reduce(f32[24,2]{0,1:T(2,128)S(1)} %broadcast_multiply_fusion.2), channel_id=1, replica_groups=mesh['tp'=8,'dp'=4] {'tp'}, use_global_device_ids=true, to_apply=%region_16.19 | all-reduce | flops 48 | bytes 384 | tf_op jit(solution)/shard_map/psum | solution.py:135
  310.4 5.2 %all_gather.27 = bf16[96,64]{1,0:T(8,128)(2,1)S(1)} all-gather(bf16[24,64]{1,0:T(8,128)(2,1)S(1)} %multiply_convert_fusion.2), channel_id=1, replica_groups=mesh['tp'=8,'dp'=4] {'dp'}, dimensions={0}, use_global_device_ids=true | all-gather | bytes 15360 | tf_op jit(solution)/shard_map/all_gather | solution.py:145
  315.6 0.1 fusion.27
  315.7 19.6 %fusion = f32[16,256]{1,0:T(8,128)S(1)} fusion(f32[96,256]{1,0:T(8,128)S(1)} %fusion.27), kind=kCustom, calls=%all-reduce-scatter | all-reduce-scatter fusion | flops 32769 | bytes 115200
  335.3 2.2 collective-permute-start
  337.5 0.6 multiply_add_fusion.1
  338.3 1.3 collective-permute-start.1
  339.6 1.2 pad_maximum_fusion
  340.8 0.6 pad_maximum_fusion.1
  341.4 0.6 pad_maximum_fusion.2
  342.1 0.6 pad_maximum_fusion.3
  342.7 0.2 concatenate.34
  343.0 0.6 constant_dynamic-slice_fusion
  (67 shorter events, 2.1 us)
Async XLA Ops:
  7.2 57.6 %copy-start.6 = (u32[32]{0:T(128)S(1)}, u32[32]{0:T(128)}, u32[]{:S(2)}) copy-start(u32[32]{0:T(128)} %constant.153) | copy-start | bytes 388
  7.2 58.7 %copy-start.1 = (bf16[2,24,3,32]{3,1,2,0:T(8,128)(2,1)S(1)}, bf16[2,24,3,32]{3,1,2,0:T(8,128)(2,1)}, u32[]{:S(2)}) copy-start(bf16[2,24,3,32]{3,1,2,0:T(8,128)(2,1)} %param.42) | copy-start | bytes 27652
  7.2 58.7 %copy-start.2 = (bf16[2,24,3,32]{3,1,2,0:T(8,128)(2,1)S(1)}, bf16[2,24,3,32]{3,1,2,0:T(8,128)(2,1)}, u32[]{:S(2)}) copy-start(bf16[2,24,3,32]{3,1,2,0:T(8,128)(2,1)} %param.43) | copy-start | bytes 27652
  7.2 64.8 %reduce-scatter.5.cloned.1.call-start = ((), (), s32[]{:S(2)}) async-start(), calls=%async_computation.2 | async-start | bytes 122880 | tf_op jit(solution)/shard_map/reduce_scatter | solution.py:90
  47.9 87.9 %copy-start = (f32[2,24,1,64,128]{4,3,2,1,0:T(8,128)S(1)}, f32[2,24,1,64,128]{4,3,2,1,0:T(8,128)}, u32[]{:S(2)}) copy-start(f32[2,24,1,64,128]{4,3,2,1,0:T(8,128)} %param.40) | copy-start | bytes 4718596
  51.1 172.0 %reduce-scatter.7.cloned.1.call-start = ((), (), s32[]{:S(2)}) async-start(), calls=%async_computation.3 | async-start | bytes 122880 | tf_op jit(solution)/shard_map/reduce_scatter | solution.py:90
  64.7 99.9 %copy-start.3 = (bf16[2,64,256]{2,1,0:T(8,128)(2,1)S(1)}, bf16[2,64,256]{2,1,0:T(8,128)(2,1)}, u32[]{:S(2)}) copy-start(bf16[2,64,256]{2,1,0:T(8,128)(2,1)} %param.39) | copy-start | bytes 196612
  72.0 62.8 %copy-start.4 = (f32[24,193]{1,0:T(8,128)S(1)}, f32[24,193]{1,0:T(8,128)}, u32[]{:S(2)}) copy-start(f32[24,193]{1,0:T(8,128)} %reduce-scatter.5.cloned.1.call-done) | copy-start | bytes 55588
  223.1 62.6 %copy-start.5 = (f32[24,193]{1,0:T(8,128)S(1)}, f32[24,193]{1,0:T(8,128)}, u32[]{:S(2)}) copy-start(f32[24,193]{1,0:T(8,128)} %reduce-scatter.7.cloned.1.call-done) | copy-start | bytes 55588
  335.3 7.4 %collective-permute-start = (f32[16,256]{1,0:T(8,128)S(1)}, f32[16,256]{1,0:T(8,128)S(1)}, u32[]{:S(2)}, u32[]{:S(2)}) collective-permute-start(f32[16,256]{1,0:T(8,128)S(1)} %fusion), channel_id=1, source_target_pairs={{0,4},{4,8},{8,12},{12,16},{16,20},{20,24},{24,28},{1,5},{5,9},{9,... | collective-permute-start | bytes 49160
  338.3 4.4 %collective-permute-start.1 = (f32[12,256]{1,0:T(8,128)S(1)}, f32[12,256]{1,0:T(8,128)S(1)}, u32[]{:S(2)}, u32[]{:S(2)}) collective-permute-start(f32[12,256]{1,0:T(8,128)S(1)} %slice.308), channel_id=1, source_target_pairs={{0,8},{4,12},{8,16},{12,20},{16,24},{20,28},{1,9},{5,13},{9,17},{1... | collective-permute-start | bytes 36872
Sparse Core Ops, SparseCore 0:
  51.2 20.7 reduce-scatter.4
  205.6 17.4 reduce-scatter.6
where the time goes:
time: 352 us; the launch traced here: 350 us
  blocking collectives  272 us (77%)
  waiting for transfers between devices  23.6 us (7%)
  local copies, waits for them, and re-layouts  16.5 us (5%)
  between operations  16.3 us (5%)
  other arithmetic  13.3 us (4%)
  matrix products  4.81 us (1%)
  starting transfers between devices  3.57 us (1%)
    all_gather x2, blocking collectives, body(): lax.all_gather(read_act, 'tp', axis=1, tiled=True)  61.1 us
    all_gather x2, blocking collectives, body(): lax.all_gather(write_act, 'tp', axis=1, tiled=True)  60.9 us
    psum x2, blocking collectives, body(): group_total = lax.psum(group_squares, 'tp')  42.6 us
    psum x1, blocking collectives, body(): lax.psum(partial_value, 'tp').astype(jnp.bfloat16)  33.8 us
    all_gather x1, blocking collectives, body(): lax.all_gather(tokens, 'tp', axis=0, tiled=True).astype(jnp.float32)  32.5 us
    reduce_scatter x2, waiting for transfers between devices, body(): lax.psum_scatter(project(), 'dp', scatter_dimension=0, tiled=True)  23.6 us
    unnamed x1, blocking collectives  19.6 us
    psum x2, blocking collectives, body(): total_sq = lax.psum(row_squares, 'dp')  11.7 us
  transfers between devices with their start and end apart: 4, of which 2 were waited for; matrix products, arithmetic and copies ran while one was open for 5% of the time, Pallas kernels for 0%

commit v1 on v0

v1 whole, which is shorter than its diff:
```python
import functools

import jax
import jax.numpy as jnp
from jax import lax
from jax.experimental import pallas as pl
from jax.experimental.pallas import tpu as pltpu
from jax.sharding import PartitionSpec as P

GROUPS = 2
norm_eps = 1e-05
MESH = pl.DeviceIdType.MESH
VMEM = pltpu.VMEM
LANES = 128
TOK, WR0, CONV, GAIN, OUT0, WR1, OUT1 = range(7)
F32 = jnp.float32
BF16 = jnp.bfloat16

NT = (((1,), (1,)), ((), ()))
NN = (((1,), (0,)), ((), ()))


def dot(a, b, dims=NN, **kw):
    return lax.dot_general(a, b, dims, preferred_element_type=F32, **kw)


def sigmoid_mul(x):
    return x * (1.0 / (1.0 + jnp.exp(-x)))


def iota(shape, axis):
    return lax.broadcasted_iota(jnp.int32, shape, axis)


def live_columns(lengths, seq, hist_len):
    row = jnp.broadcast_to(lengths.astype(F32), (seq, seq))
    same = iota((seq, seq), 0) == iota((seq, seq), 1)
    column = jnp.sum(jnp.where(same, row, 0.0), axis=1, keepdims=True)
    return [(column >= float(hist_len - k)).astype(F32) for k in range(hist_len)]


def mixer_kernel(
    tp, dp, tokens, lengths, norm_gain, w_gate, w_value, w_write, w_read, w_step,
    step_bias, decay_rate, skip_gain, tap_value, tap_write, tap_read, group_gain,
    w_out, state, hist_value, hist_write, hist_read,
    mixed, aux, fresh,
    tok_buf, wr_send, wr_buf, conv_send, conv_buf, gain_send, gain_buf, out_buf,
    local_w, cur, rs_send, rs_buf, mix_send, mix_buf, last_buf, st, stb,
    tp_send, tp_recv, rs_ssem, rs_rsem, mix_ssem, mix_rsem, last_ssem, last_rsem, st_sem,
):
    t = lax.axis_index("tp")
    d = lax.axis_index("dp")
    rows = tokens.shape[0]
    hist_len, seq, vcols = hist_value.shape[1:]
    wcols = w_write.shape[1]
    cj = wcols // GROUPS
    nstate = state.shape[-1]
    hdim = state.shape[-2]
    feats = tokens.shape[1]
    total = feats * dp
    seqs = seq * dp
    per_group = tp // GROUPS
    group = t // per_group
    k_blocks = tp // dp
    packed = mix_send.shape[1]
    lane = iota((1, LANES), 1)
    low = lane < hdim

    barrier = pltpu.get_barrier_semaphore()
    for i in range(1, tp):
        pl.semaphore_signal(barrier, inc=1, device_id={"tp": lax.rem(t + i, tp), "dp": d}, device_id_type=MESH)
    for i in range(1, dp):
        pl.semaphore_signal(barrier, inc=1, device_id={"tp": t, "dp": lax.rem(d + i, dp)}, device_id_type=MESH)
    st_copy = pltpu.make_async_copy(state, st, st_sem)
    st_copy.start()

    size = 2 * wcols
    r, c = iota((size, size), 0), iota((size, size), 1)
    source = ((r // cj) % 2) * wcols + (r % cj) * GROUPS + r // (2 * cj)
    pick = (c == source).astype(F32)
    pick16 = pick.astype(BF16)
    live = live_columns(lengths[...], seq, hist_len)
    for l in range(2):
        both = jnp.concatenate([w_write[l], w_read[l]], axis=0)
        got = dot(pick16, both).astype(BF16)
        for g in range(GROUPS):
            for kind in range(2):
                at = (g * 2 + kind) * cj
                wr_send[l, g, kind] = got[at:at + cj]

    pl.semaphore_wait(barrier, tp + dp - 2)
    sent = []

    def spread(cat, src_of, dst):
        out = []
        for i in range(1, tp):
            to = lax.rem(t + i, tp)
            copy = pltpu.make_async_remote_copy(
                src_ref=src_of(to), dst_ref=dst, send_sem=tp_send.at[cat, i - 1],
                recv_sem=tp_recv.at[cat, i - 1], device_id={"tp": to, "dp": d}, device_id_type=MESH)
            copy.start()
            out.append(copy)
        sent.extend(out)
        return out

    got_tok = spread(TOK, lambda to: tokens, tok_buf.at[t])
    got_wr = [spread(WR0, lambda to: wr_send.at[0, to // per_group], wr_buf.at[0, :, t]), None]

    pieces = []
    for l in range(2):
        parts = []
        for hist, tap in ((hist_write, tap_write), (hist_read, tap_read)):
            total_c = sum(hist[l, k].astype(F32) * live[k] * tap[l, k:k + 1] for k in range(hist_len))
            last = tap[l, hist_len:hist_len + 1]
            parts.append(jnp.concatenate([total_c, last, jnp.zeros((7, wcols), F32)], axis=0))
        pieces.append(jnp.concatenate(parts, axis=1))
    span = seq + 8
    pieces.append(jnp.zeros((LANES - 2 * span, size), F32))
    moved = dot(pick, jnp.concatenate(pieces, axis=0), NT, precision=lax.Precision.HIGHEST)
    for g in range(GROUPS):
        for kind in range(2):
            at = (g * 2 + kind) * cj
            conv_send[g, kind] = moved[at:at + cj]
    gg = group_gain[...]
    gain_send[...] = jnp.concatenate([jnp.concatenate([gg, gg], axis=1), jnp.zeros((6, LANES), F32)], axis=0)
    got_conv = spread(CONV, lambda to: conv_send.at[to // per_group], conv_buf.at[:, t])
    got_gain = spread(GAIN, lambda to: gain_send, gain_buf.at[t])
    got_out = [spread(OUT0, lambda to: w_out.at[0], out_buf.at[0, t]), None]
    got_wr[1] = spread(WR1, lambda to: wr_send.at[1, to // per_group], wr_buf.at[1, :, t])
    got_out[1] = spread(OUT1, lambda to: w_out.at[1], out_buf.at[1, t])

    tok_buf[t] = tokens[...]
    conv_buf[:, t] = conv_send[group]
    gain_buf[t] = gain_send[...]
    for l in range(2):
        wr_buf[l, :, t] = wr_send[l, group]
        out_buf[l, t] = w_out[l]
        local_w[l, 0] = jnp.concatenate([w_value[l], w_gate[l]], axis=0)
        local_w[l, 1] = jnp.concatenate(
            [w_write[l], w_read[l], w_step[l:l + 1], jnp.zeros((LANES - size - 1, feats), BF16)], axis=0)
    st_copy.wait()
    for l in range(2):
        stb[l] = st[l].reshape(seq * hdim, nstate).astype(BF16)

    for copy in got_tok:
        copy.wait_recv()
    for i in range(tp):
        cur[i * rows:(i + 1) * rows] = tok_buf[i].astype(F32)

    def pair_rows(get, p):
        a, b = get(2 * p).astype(F32), get(2 * p + 1).astype(F32)
        ra, rb = pltpu.roll(a, hdim, 1), pltpu.roll(b, hdim, 1)
        cut = 2 * packed - seq
        return jnp.concatenate([jnp.where(low, a, rb), jnp.where(low, ra, b)[cut:]], axis=0)

    def normed_rows(get, l):
        cols = [pair_rows(get, p) for p in range(tp // 2)]
        pairs = tp // 2 // GROUPS
        done = []
        for g in range(GROUPS):
            own = cols[g * pairs:(g + 1) * pairs]
            sq = sum(jnp.sum(x * x, axis=1, keepdims=True) for x in own)
            scale = lax.rsqrt(sq / (per_group * hdim) + norm_eps)
            for p, x in enumerate(own):
                at = 2 * (g * pairs + p)
                gain = jnp.where(low, gain_buf[at, l:l + 1], gain_buf[at + 1, l:l + 1])
                done.append((x * scale * gain).astype(BF16))
        return jnp.concatenate(done, axis=1)

    for l in range(2):
        value = cur[...]
        x = (value * norm_gain[l:l + 1]).astype(BF16)
        squares = jnp.sum(value * value, axis=1, keepdims=True)
        first = dot(x, local_w[l, 0], NT)
        last = dot(x, local_w[l, 1], NT)
        last = jnp.where(lane == size + 1, squares, last)
        for j in range(dp):
            rs_send[l, j, :, 0:LANES] = first[j * seq:(j + 1) * seq].astype(BF16)
            rs_send[l, j, :, 3 * LANES:] = last[j * seq:(j + 1) * seq].astype(BF16)
        for copy in got_wr[l]:
            copy.wait_recv()
        for kind in range(2):
            mid = dot(x, wr_buf[l, kind].reshape(nstate, feats), NT)
            for j in range(dp):
                rs_send[l, j, :, (1 + kind) * LANES:(2 + kind) * LANES] = mid[j * seq:(j + 1) * seq].astype(BF16)
        got = []
        for i in range(1, dp):
            to = lax.rem(d + i, dp)
            copy = pltpu.make_async_remote_copy(
                src_ref=rs_send.at[l, to], dst_ref=rs_buf.at[l, d], send_sem=rs_ssem.at[l, i - 1],
                recv_sem=rs_rsem.at[l, i - 1], device_id={"tp": t, "dp": to}, device_id_type=MESH)
            copy.start()
            got.append(copy)
        sent.extend(got)
        rs_buf[l, d] = rs_send[l, d]
        value_hist = sum(
            hist_value[l, k].astype(F32) * live[k] * tap_value[l, k:k + 1] for k in range(hist_len))
        if l == 0:
            for copy in got_conv + got_gain:
                copy.wait_recv()
            convs = [conv_buf[kind].reshape(nstate, LANES).T for kind in range(2)]
        for copy in got:
            copy.wait_recv()
        z = sum(rs_buf[l, j].astype(F32) for j in range(dp))
        z = z * lax.rsqrt(z[:, 3 * LANES + size + 1:3 * LANES + size + 2] / total + norm_eps)
        step_raw = z[:, 3 * LANES + size:3 * LANES + size + 1]
        z16 = z.astype(BF16)
        zr = z16.astype(F32)
        fresh[l, :, 0:LANES] = z16[:, 0:LANES]
        fresh[l, :, LANES:] = z16[:, 3 * LANES:]
        acts = []
        for kind in range(2):
            base = convs[kind][l * span:l * span + seq]
            tap = convs[kind][l * span + seq:l * span + seq + 1]
            acts.append(sigmoid_mul(base + tap * zr[:, (1 + kind) * LANES:(2 + kind) * LANES]))
        write, read = acts
        u = sigmoid_mul(value_hist + tap_value[l, hist_len:hist_len + 1] * zr[:, 0:vcols])
        gate = zr[:, vcols:2 * vcols]
        pre = step_raw + step_bias[0, l]
        step = jnp.maximum(pre, 0.0) + jnp.log1p(jnp.exp(-jnp.abs(pre)))
        keep = jnp.exp(-decay_rate[0, l] * step)
        read16 = read.astype(BF16)
        held = jnp.zeros((seq, 2 * hdim), F32)
        which = iota((seq, 1), 0)
        for j in range(seq // 2):
            part = dot(read16, stb[l, 2 * j * hdim:2 * (j + 1) * hdim, :], NT)
            held = jnp.where(which // 2 == j, part, held)
        held = jnp.where(which % 2 == 0, held[:, :hdim], held[:, hdim:])
        su = step * u
        overlap = jnp.sum(write * read, axis=1, keepdims=True)
        readout = keep * held + su * overlap + skip_gain[0, l] * u
        gated = readout * sigmoid_mul(gate)
        aux[l, :, 0:nstate] = write
        aux[l, :, nstate:] = jnp.concatenate([su, jnp.broadcast_to(keep, (seq, hdim))], axis=1)
        mix_send[l] = jnp.concatenate([gated[:packed], gated[seq - packed:]], axis=1).astype(BF16)
        if l == 0:
            got = []
            for j in range(dp):
                for i in range(tp):
                    if i + j == 0:
                        continue
                    copy = pltpu.make_async_remote_copy(
                        src_ref=mix_send.at[0], dst_ref=mix_buf.at[d, t],
                        send_sem=mix_ssem.at[j * tp + i - 1], recv_sem=mix_rsem.at[j * tp + i - 1],
                        device_id={"tp": lax.rem(t + i, tp), "dp": lax.rem(d + j, dp)}, device_id_type=MESH)
                    copy.start()
                    got.append(copy)
            sent.extend(got)
            mix_buf[d, t] = mix_send[0]
            for copy in got_out[0]:
                copy.wait_recv()
            for copy in got:
                copy.wait_recv()
            lhs = jnp.concatenate(
                [normed_rows(lambda i, j=j: mix_buf[j, i], 0) for j in range(dp)], axis=0)
            full = dot(lhs, out_buf[0].reshape(tp * vcols, feats))
            cur[...] = full.astype(BF16).astype(F32)

    def last_copy(j, m):
        to = k_blocks * d + m
        return to, pltpu.make_async_remote_copy(
            src_ref=mix_send.at[1], dst_ref=last_buf.at[t], send_sem=last_ssem.at[j * k_blocks + m],
            recv_sem=last_rsem.at[t], device_id={"tp": to, "dp": lax.rem(d + j, dp)}, device_id_type=MESH)

    for j in range(dp):
        for m in range(k_blocks):
            to, copy = last_copy(j, m)
            if j == 0:
                pl.when(to != t)(copy.start)
            else:
                copy.start()
    for copy in got_out[1]:
        copy.wait_recv()

    def arrived(i):
        pltpu.make_async_remote_copy(
            src_ref=mix_send.at[1], dst_ref=last_buf.at[i], send_sem=last_ssem.at[0],
            recv_sem=last_rsem.at[i], device_id={"tp": t, "dp": lax.rem(d + 1, dp)},
            device_id_type=MESH).wait_recv()

    for i in range(1, tp):
        arrived(lax.rem(t + i, tp))
    is_mine = t // k_blocks == d
    pl.when(jnp.logical_not(is_mine))(lambda: arrived(t))

    @pl.when(is_mine)
    def _():
        last_buf[t] = mix_send[1]

    full = dot(normed_rows(lambda i: last_buf[i], 1), out_buf[1].reshape(tp * vcols, feats))
    mine = full[:rows]
    for m in range(1, k_blocks):
        mine = jnp.where(t % k_blocks == m, full[m * rows:(m + 1) * rows], mine)
    mixed[...] = mine

    for copy in sent:
        copy.wait_send()
    for j in range(dp):
        for m in range(k_blocks):
            to, copy = last_copy(j, m)
            if j == 0:
                pl.when(to != t)(copy.wait_send)
            else:
                copy.wait_send()


def finish_kernel(lengths, mixed_in, aux, fresh, state, hist_value, hist_write, hist_read,
                  mixed, new_state, new_value, new_write, new_read):
    hist_len, seq, vcols = hist_value.shape[1:]
    wcols = hist_write.shape[-1]
    nstate = state.shape[-1]
    hdim = state.shape[-2]
    l = pl.program_id(0)
    live = live_columns(lengths[...], seq, hist_len)
    mixed[...] = mixed_in[...]
    edges = (
        (hist_value, new_value, 0, vcols),
        (hist_write, new_write, LANES, wcols),
        (hist_read, new_read, LANES + wcols, wcols),
    )
    for old, new, at, width in edges:
        for k in range(1, hist_len):
            new[0, k - 1] = (old[0, k].astype(F32) * live[k]).astype(BF16)
        new[0, hist_len - 1] = fresh[0, :, at:at + width]
    write = aux[0, :, 0:nstate]
    rest = aux[0, :, nstate:].T
    for s in range(seq):
        su = rest[0:hdim, s:s + 1]
        keep = rest[hdim:, s:s + 1]
        new_state[0, s] = keep * state[0, s] + su * write[s:s + 1]


def body(tp, dp, tokens, lengths, norm_gain, w_gate, w_value, w_write, w_read, w_step, step_bias,
         decay_rate, skip_gain, conv_value_w, conv_write_w, conv_read_w, group_gain, w_out, state,
         hist_value, hist_write, hist_read):
    rows, feats = tokens.shape
    seq = state.shape[1]
    hdim, nstate = state.shape[3:]
    hist_len = hist_value.shape[2]
    vcols, wcols = w_value.shape[2], w_write.shape[2]
    cj = wcols // GROUPS
    packed = 16
    lens = lengths.reshape(1, seq)
    flip = functools.partial(jnp.swapaxes, axis1=1, axis2=2)
    state4 = state.reshape(2, seq, hdim, nstate)
    hists = [flip(h) for h in (hist_value, hist_write, hist_read)]
    vspec = pl.BlockSpec(memory_space=VMEM)
    sspec = pl.BlockSpec(memory_space=pltpu.SMEM)
    aspec = pl.BlockSpec(memory_space=pl.ANY)
    dma = pltpu.SemaphoreType.DMA
    mixed, aux, fresh = pl.pallas_call(
        functools.partial(mixer_kernel, tp, dp),
        out_shape=(
            jax.ShapeDtypeStruct((rows, feats), F32),
            jax.ShapeDtypeStruct((2, seq, nstate + 2 * hdim), F32),
            jax.ShapeDtypeStruct((2, seq, 2 * LANES), BF16),
        ),
        in_specs=[vspec] * 8 + [sspec] * 3 + [vspec] * 5 + [aspec] + [vspec] * 3,
        out_specs=(vspec,) * 3,
        scratch_shapes=[
            VMEM((tp, rows, feats), BF16),
            VMEM((2, GROUPS, 2, cj, feats), BF16),
            VMEM((2, 2, tp, cj, feats), BF16),
            VMEM((GROUPS, 2, cj, LANES), F32),
            VMEM((2, tp, cj, LANES), F32),
            VMEM((8, LANES), F32),
            VMEM((tp, 8, LANES), F32),
            VMEM((2, tp, vcols, feats), BF16),
            VMEM((2, 2, LANES, feats), BF16),
            VMEM((seq * dp, feats), F32),
            VMEM((2, dp, seq, 4 * LANES), BF16),
            VMEM((2, dp, seq, 4 * LANES), BF16),
            VMEM((2, packed, LANES), BF16),
            VMEM((dp, tp, packed, LANES), BF16),
            VMEM((tp, packed, LANES), BF16),
            VMEM((2, seq, hdim, nstate), F32),
            VMEM((2, seq * hdim, nstate), BF16),
            dma((7, tp - 1)),
            dma((7, tp - 1)),
            dma((2, dp - 1)),
            dma((2, dp - 1)),
            dma((tp * dp - 1,)),
            dma((tp * dp - 1,)),
            dma((tp,)),
            dma((tp,)),
            dma,
        ],
        compiler_params=pltpu.CompilerParams(
            collective_id=0, has_side_effects=True, vmem_limit_bytes=40 * 1024 * 1024),
        name="mixer_blocks",
    )(tokens, lens, norm_gain, flip(w_gate), flip(w_value), flip(w_write), flip(w_read),
      jnp.transpose(w_step, (2, 0, 1)).reshape(2, feats), step_bias.T, decay_rate.T, skip_gain.T,
      conv_value_w, conv_write_w, conv_read_w, group_gain, w_out, state4, *hists)

    def whole(shape):
        return pl.BlockSpec(shape, lambda l: (0,) * len(shape))

    def layer(shape):
        return pl.BlockSpec((1,) + shape[1:], lambda l: (l,) + (0,) * (len(shape) - 1))

    mixed, new_state, *fresh_hists = pl.pallas_call(
        finish_kernel,
        grid=(2,),
        out_shape=(
            jax.ShapeDtypeStruct(mixed.shape, F32),
            jax.ShapeDtypeStruct(state4.shape, F32),
            *[jax.ShapeDtypeStruct(h.shape, BF16) for h in hists],
        ),
        in_specs=[whole(lens.shape), whole(mixed.shape), layer(aux.shape), layer(fresh.shape),
                  layer(state4.shape), *[layer(h.shape) for h in hists]],
        out_specs=(whole(mixed.shape), layer(state4.shape), *[layer(h.shape) for h in hists]),
        name="new_states",
    )(lens, mixed, aux, fresh, state4, *hists)
    return (mixed, new_state.reshape(state.shape), *[flip(h) for h in fresh_hists])


def solution(mesh):
    columns = P(None, "dp", "tp")
    heads = P(None, "tp")
    taps = P(None, None, "tp")
    states = P(None, "dp", "tp", None, None)
    history = P(None, "dp", None, "tp")
    in_specs = (
        P("tp", "dp"), P("dp"), P(None, "dp"), columns, columns, columns, columns, columns,
        heads, heads, heads, taps, taps, taps, heads, P(None, "tp", "dp"), states,
        history, history, history,
    )
    out_specs = (P("tp", "dp"), states, history, history, history)
    run = functools.partial(body, mesh.shape["tp"], mesh.shape["dp"])
    return jax.shard_map(run, mesh=mesh, in_specs=in_specs, out_specs=out_specs, check_vma=False)
```

time: 352 us -> 65.9 us (0.19)
  blocking collectives: 272 us -> 0 us
  Pallas kernels: 0 us -> 47.4 us
  waiting for transfers between devices: 23.6 us -> 0 us
  between operations: 16.3 us -> 0.68 us
  other arithmetic: 13.3 us -> 0 us
  matrix products: 4.81 us -> 0 us
  starting transfers between devices: 3.57 us -> 0 us
    all_gather x7 -> x0, blocking collectives: 165 us -> none  [the longest x2 61.1 us: body(): lax.all_gather(read_act, 'tp', axis=1, tiled=True)]
    psum x5 -> x0, blocking collectives: 88 us -> none  [the longest x2 42.6 us: body(): group_total = lax.psum(group_squares, 'tp')]
    pallas_call x0 -> x2, Pallas kernels: none -> 47.4 us  [the longest x1 44 us: body(): pl.pallas_call(functools.partial(mixer_kernel, tp, dp), out_shape=(jax.Sh...]
    reduce_scatter x2 -> x0, waiting for transfers between devices: 23.6 us -> none  [body(): lax.psum_scatter(project(), 'dp', scatter_dimension=0, tiled=True)]
    unnamed x1 -> x0, blocking collectives: 19.6 us -> none
    unnamed x30 -> x46, local copies, waits for them, and re-layouts: 5.4 us -> 17 us
    mul x9 -> x0, local copies, waits for them, and re-layouts: 5.08 us -> none  [the longest x3 2.1 us: conv_update(): current.astype(jnp.float32) * conv_taps[-1][None, :]]
    dot_general x6 -> x0, matrix products: 4.81 us -> none  [the longest x2 2.88 us: body(): jnp.einsum('shpn,shn->shp', updated, read_heads, precision=lax.Precision....]
  transfers between devices with their start and end apart: 4 -> 0, of which waited for: 2 -> 0; matrix products, arithmetic and copies ran while one was open for 5% -> 0% of each run, Pallas kernels for 0% -> 0%
where the time goes in v1:
time: 65.9 us; the launch traced here: 65 us
  Pallas kernels  47.4 us (72%)
  local copies, waits for them, and re-layouts  17 us (26%)
  between operations  0.68 us (1%)
    pallas_call x1, Pallas kernels, body(): pl.pallas_call(functools.partial(mixer_kernel, tp, dp), out_shape=(jax.Sh...  44 us
    unnamed x46, local copies, waits for them, and re-layouts  17 us
    pallas_call x1, Pallas kernels, body(): pl.pallas_call(finish_kernel, grid=(2,), out_shape=(jax.ShapeDtypeStruct(...  3.33 us

profile of v1, /device:TPU:0, one launch (start us, length us, event | category | flops | bytes accessed | tf_op | source)
XLA Modules:
  0.0 65.0 jit_solution(13511309678583934933)
XLA Ops:
  0.6 0.0 copy-start
  0.6 1.4 %copy-done = f32[2,24,1,64,128]{4,3,2,1,0:T(8,128)S(1)} copy-done((f32[2,24,1,64,128]{4,3,2,1,0:T(8,128)S(1)}, f32[2,24,1,64,128]{4,3,2,1,0:T(8,128)}, u32[]{:S(2)}) %copy-start) | copy-done | bytes 1572888
  2.0 0.0 copy-start.1
  2.1 0.8 %copy-done.1 = bf16[2,24,3,64]{3,1,2,0:T(8,128)(2,1)S(1)} copy-done((bf16[2,24,3,64]{3,1,2,0:T(8,128)(2,1)S(1)}, bf16[2,24,3,64]{3,1,2,0:T(8,128)(2,1)}, u32[]{:S(2)}) %copy-start.1) | copy-done | bytes 18456
  2.8 0.0 copy-start.2
  2.8 0.8 %copy-done.2 = bf16[2,24,3,32]{3,1,2,0:T(8,128)(2,1)S(1)} copy-done((bf16[2,24,3,32]{3,1,2,0:T(8,128)(2,1)S(1)}, bf16[2,24,3,32]{3,1,2,0:T(8,128)(2,1)}, u32[]{:S(2)}) %copy-start.2) | copy-done | bytes 9240
  3.6 0.0 copy-start.3
  3.6 0.8 %copy-done.3 = bf16[2,24,3,32]{3,1,2,0:T(8,128)(2,1)S(1)} copy-done((bf16[2,24,3,32]{3,1,2,0:T(8,128)(2,1)S(1)}, bf16[2,24,3,32]{3,1,2,0:T(8,128)(2,1)}, u32[]{:S(2)}) %copy-start.3) | copy-done | bytes 9240
  4.4 0.0 copy-start.4
  4.4 0.8 %copy-done.4 = bf16[2,256,64]{1,2,0:T(8,128)(2,1)S(1)} copy-done((bf16[2,256,64]{1,2,0:T(8,128)(2,1)S(1)}, bf16[2,256,64]{1,2,0:T(8,128)(2,1)}, u32[]{:S(2)}) %copy-start.4) | copy-done | bytes 65560
  5.2 0.0 copy-start.5
  5.2 0.8 %copy-done.5 = bf16[2,256,64]{1,2,0:T(8,128)(2,1)S(1)} copy-done((bf16[2,256,64]{1,2,0:T(8,128)(2,1)S(1)}, bf16[2,256,64]{1,2,0:T(8,128)(2,1)}, u32[]{:S(2)}) %copy-start.5) | copy-done | bytes 65560
  6.0 0.0 copy-start.6
  6.0 0.8 %copy-done.6 = bf16[2,64,256]{2,1,0:T(8,128)(2,1)S(1)} copy-done((bf16[2,64,256]{2,1,0:T(8,128)(2,1)S(1)}, bf16[2,64,256]{2,1,0:T(8,128)(2,1)}, u32[]{:S(2)}) %copy-start.6) | copy-done | bytes 65560
  6.9 0.0 copy-start.8
  6.9 0.8 %copy-done.8 = bf16[2,256,32]{1,2,0:T(8,128)(2,1)S(1)} copy-done((bf16[2,256,32]{1,2,0:T(8,128)(2,1)S(1)}, bf16[2,256,32]{1,2,0:T(8,128)(2,1)}, u32[]{:S(2)}) %copy-start.8) | copy-done | bytes 32792
  7.6 0.0 copy-start.9
  7.6 0.8 %copy-done.9 = bf16[2,256,32]{1,2,0:T(8,128)(2,1)S(1)} copy-done((bf16[2,256,32]{1,2,0:T(8,128)(2,1)S(1)}, bf16[2,256,32]{1,2,0:T(8,128)(2,1)}, u32[]{:S(2)}) %copy-start.9) | copy-done | bytes 32792
  8.4 0.0 copy-start.12
  8.4 0.7 %copy-done.12 = bf16[12,256]{1,0:T(8,128)(2,1)S(1)} copy-done((bf16[12,256]{1,0:T(8,128)(2,1)S(1)}, bf16[12,256]{1,0:T(8,128)(2,1)}, u32[]{:S(2)}) %copy-start.12) | copy-done | bytes 6168
  9.1 0.0 copy-start.13
  9.1 0.7 %copy-done.13 = f32[2,4,64]{2,1,0:T(4,128)S(1)} copy-done((f32[2,4,64]{2,1,0:T(4,128)S(1)}, f32[2,4,64]{2,1,0:T(4,128)}, u32[]{:S(2)}) %copy-start.13) | copy-done | bytes 2072
  9.8 0.0 copy-start.14
  9.8 0.7 %copy-done.14 = f32[2,4,32]{2,1,0:T(4,128)S(1)} copy-done((f32[2,4,32]{2,1,0:T(4,128)S(1)}, f32[2,4,32]{2,1,0:T(4,128)}, u32[]{:S(2)}) %copy-start.14) | copy-done | bytes 1048
  10.5 0.0 copy-start.15
  10.5 0.7 %copy-done.15 = f32[2,4,32]{2,1,0:T(4,128)S(1)} copy-done((f32[2,4,32]{2,1,0:T(4,128)S(1)}, f32[2,4,32]{2,1,0:T(4,128)}, u32[]{:S(2)}) %copy-start.15) | copy-done | bytes 1048
  11.2 0.0 copy-start.16
  11.2 0.7 %copy-done.16 = f32[2,256]{1,0:T(2,128)S(1)} copy-done((f32[2,256]{1,0:T(2,128)S(1)}, f32[2,256]{1,0:T(2,128)}, u32[]{:S(2)}) %copy-start.16) | copy-done | bytes 2072
  11.8 0.0 copy-start.17
  11.8 0.7 %copy-done.17 = s32[24]{0:T(128)S(1)} copy-done((s32[24]{0:T(128)S(1)}, s32[24]{0:T(128)}, u32[]{:S(2)}) %copy-start.17) | copy-done | bytes 120
  12.5 0.0 copy-start.18
  12.5 0.7 %copy-done.18 = bf16[2,256,1]{1,0,2:T(2,128)(2,1)S(1)} copy-done((bf16[2,256,1]{1,0,2:T(2,128)(2,1)S(1)}, bf16[2,256,1]{1,0,2:T(2,128)(2,1)}, u32[]{:S(2)}) %copy-start.18) | copy-done | bytes 1048
  13.2 0.0 copy-start.19
  13.2 0.7 %copy-done.19 = f32[2,64]{1,0:T(2,128)S(1)} copy-done((f32[2,64]{1,0:T(2,128)S(1)}, f32[2,64]{1,0:T(2,128)}, u32[]{:S(2)}) %copy-start.19) | copy-done | bytes 536
  13.8 0.0 copy-start.20
  13.8 0.7 %copy-done.20 = f32[2,1]{0,1:T(1,128)S(1)} copy-done((f32[2,1]{0,1:T(1,128)S(1)}, f32[2,1]{0,1:T(1,128)}, u32[]{:S(2)}) %copy-start.20) | copy-done | bytes 32
  14.5 0.0 copy-start.21
  14.5 0.7 %copy-done.21 = f32[2,1]{0,1:T(1,128)S(1)} copy-done((f32[2,1]{0,1:T(1,128)S(1)}, f32[2,1]{0,1:T(1,128)}, u32[]{:S(2)}) %copy-start.21) | copy-done | bytes 32
  15.2 0.0 copy-start.22
  15.2 0.7 %copy-done.22 = f32[2,1]{0,1:T(1,128)S(1)} copy-done((f32[2,1]{0,1:T(1,128)S(1)}, f32[2,1]{0,1:T(1,128)}, u32[]{:S(2)}) %copy-start.22) | copy-done | bytes 32
  15.8 44.0 %mixer_blocks.1 = (f32[12,256]{1,0:T(8,128)S(1)}, f32[2,24,256]{2,1,0:T(8,128)S(1)}, bf16[2,24,256]{2,1,0:T(8,128)(2,1)S(1)}) custom-call(bf16[12,256]{1,0:T(8,128)(2,1)S(1)} %copy-done.12, s32[1,24]{1,0:T(1,128)S(1)} %bitcast.32, f32[2,256]{1,0:T(2,128)S(1)} %copy-done.16, bf16[2,64,256]{2,1,0:T(8,128)(2,1)S(1)} %bitcast.27, ...), custom_call_target="tpu_custom_call" | custom-call | tf_op jit(solution)/shard_map/mixer_blocks/pallas_call | solution.py:351
  59.9 0.0 copy-start.7
  59.9 0.6 copy-done.7
  60.5 0.0 copy-start.10
  60.5 0.6 copy-done.10
  61.1 0.0 copy-start.11
  61.1 0.6 copy-done.11
  61.7 3.3 %new_states.1 = (f32[12,256]{1,0:T(8,128)}, f32[2,24,64,128]{3,2,1,0:T(8,128)}, bf16[2,3,24,64]{3,2,1,0:T(8,128)(2,1)}, bf16[2,3,24,32]{3,2,1,0:T(8,128)(2,1)}, bf16[2,3,24,32]{3,2,1,0:T(8,128)(2,1)}) custom-call(s32[1,24]{1,0:T(1,128)} %bitcast.31, f32[12,256]{1,0:T(8,128)} %copy-done.11, f32[2,24,256]{2,1,0:T(8,128)} %copy-done.7, ...), custom_call_target="tpu_custom_call" | custom-call | tf_op jit(solution)/shard_map/new_states/pallas_call | solution.py:401
Async XLA Ops:
  0.6 1.4 %copy-start = (f32[2,24,1,64,128]{4,3,2,1,0:T(8,128)S(1)}, f32[2,24,1,64,128]{4,3,2,1,0:T(8,128)}, u32[]{:S(2)}) copy-start(f32[2,24,1,64,128]{4,3,2,1,0:T(8,128)} %param.36) | copy-start | bytes 4718596
  2.0 0.8 %copy-start.1 = (bf16[2,24,3,64]{3,1,2,0:T(8,128)(2,1)S(1)}, bf16[2,24,3,64]{3,1,2,0:T(8,128)(2,1)}, u32[]{:S(2)}) copy-start(bf16[2,24,3,64]{3,1,2,0:T(8,128)(2,1)} %param.37) | copy-start | bytes 55300
  2.8 0.8 %copy-start.2 = (bf16[2,24,3,32]{3,1,2,0:T(8,128)(2,1)S(1)}, bf16[2,24,3,32]{3,1,2,0:T(8,128)(2,1)}, u32[]{:S(2)}) copy-start(bf16[2,24,3,32]{3,1,2,0:T(8,128)(2,1)} %param.38) | copy-start | bytes 27652
  3.6 0.8 %copy-start.3 = (bf16[2,24,3,32]{3,1,2,0:T(8,128)(2,1)S(1)}, bf16[2,24,3,32]{3,1,2,0:T(8,128)(2,1)}, u32[]{:S(2)}) copy-start(bf16[2,24,3,32]{3,1,2,0:T(8,128)(2,1)} %param.39) | copy-start | bytes 27652
  4.4 0.8 %copy-start.4 = (bf16[2,256,64]{1,2,0:T(8,128)(2,1)S(1)}, bf16[2,256,64]{1,2,0:T(8,128)(2,1)}, u32[]{:S(2)}) copy-start(bf16[2,256,64]{1,2,0:T(8,128)(2,1)} %param.23) | copy-start | bytes 196612
  5.2 0.8 %copy-start.5 = (bf16[2,256,64]{1,2,0:T(8,128)(2,1)S(1)}, bf16[2,256,64]{1,2,0:T(8,128)(2,1)}, u32[]{:S(2)}) copy-start(bf16[2,256,64]{1,2,0:T(8,128)(2,1)} %param.24) | copy-start | bytes 196612
  6.0 0.8 %copy-start.6 = (bf16[2,64,256]{2,1,0:T(8,128)(2,1)S(1)}, bf16[2,64,256]{2,1,0:T(8,128)(2,1)}, u32[]{:S(2)}) copy-start(bf16[2,64,256]{2,1,0:T(8,128)(2,1)} %w_out.1) | copy-start | bytes 196612
  6.9 0.8 %copy-start.8 = (bf16[2,256,32]{1,2,0:T(8,128)(2,1)S(1)}, bf16[2,256,32]{1,2,0:T(8,128)(2,1)}, u32[]{:S(2)}) copy-start(bf16[2,256,32]{1,2,0:T(8,128)(2,1)} %param.25) | copy-start | bytes 98308
  7.6 0.8 %copy-start.9 = (bf16[2,256,32]{1,2,0:T(8,128)(2,1)S(1)}, bf16[2,256,32]{1,2,0:T(8,128)(2,1)}, u32[]{:S(2)}) copy-start(bf16[2,256,32]{1,2,0:T(8,128)(2,1)} %param.26) | copy-start | bytes 98308
  8.4 0.7 %copy-start.12 = (bf16[12,256]{1,0:T(8,128)(2,1)S(1)}, bf16[12,256]{1,0:T(8,128)(2,1)}, u32[]{:S(2)}) copy-start(bf16[12,256]{1,0:T(8,128)(2,1)} %tokens.1) | copy-start | bytes 18436
  9.1 0.7 %copy-start.13 = (f32[2,4,64]{2,1,0:T(4,128)S(1)}, f32[2,4,64]{2,1,0:T(4,128)}, u32[]{:S(2)}) copy-start(f32[2,4,64]{2,1,0:T(4,128)} %tap_value.1) | copy-start | bytes 6148
  9.8 0.7 %copy-start.14 = (f32[2,4,32]{2,1,0:T(4,128)S(1)}, f32[2,4,32]{2,1,0:T(4,128)}, u32[]{:S(2)}) copy-start(f32[2,4,32]{2,1,0:T(4,128)} %tap_write.1) | copy-start | bytes 3076
  10.5 0.7 %copy-start.15 = (f32[2,4,32]{2,1,0:T(4,128)S(1)}, f32[2,4,32]{2,1,0:T(4,128)}, u32[]{:S(2)}) copy-start(f32[2,4,32]{2,1,0:T(4,128)} %tap_read.1) | copy-start | bytes 3076
  11.2 0.7 %copy-start.16 = (f32[2,256]{1,0:T(2,128)S(1)}, f32[2,256]{1,0:T(2,128)}, u32[]{:S(2)}) copy-start(f32[2,256]{1,0:T(2,128)} %norm_gain.1) | copy-start | bytes 6148
  11.8 0.7 %copy-start.17 = (s32[24]{0:T(128)S(1)}, s32[24]{0:T(128)}, u32[]{:S(2)}) copy-start(s32[24]{0:T(128)} %param.21) | copy-start | bytes 292
  12.5 0.7 %copy-start.18 = (bf16[2,256,1]{1,0,2:T(2,128)(2,1)S(1)}, bf16[2,256,1]{1,0,2:T(2,128)(2,1)}, u32[]{:S(2)}) copy-start(bf16[2,256,1]{1,0,2:T(2,128)(2,1)} %param.27) | copy-start | bytes 3076
  13.2 0.7 %copy-start.19 = (f32[2,64]{1,0:T(2,128)S(1)}, f32[2,64]{1,0:T(2,128)}, u32[]{:S(2)}) copy-start(f32[2,64]{1,0:T(2,128)} %group_gain.1) | copy-start | bytes 1540
  13.8 0.7 %copy-start.20 = (f32[2,1]{0,1:T(1,128)S(1)}, f32[2,1]{0,1:T(1,128)}, u32[]{:S(2)}) copy-start(f32[2,1]{0,1:T(1,128)} %param.28) | copy-start | bytes 28
  14.5 0.7 %copy-start.21 = (f32[2,1]{0,1:T(1,128)S(1)}, f32[2,1]{0,1:T(1,128)}, u32[]{:S(2)}) copy-start(f32[2,1]{0,1:T(1,128)} %param.29) | copy-start | bytes 28
  15.2 0.7 %copy-start.22 = (f32[2,1]{0,1:T(1,128)S(1)}, f32[2,1]{0,1:T(1,128)}, u32[]{:S(2)}) copy-start(f32[2,1]{0,1:T(1,128)} %param.30) | copy-start | bytes 28
  59.9 0.6 copy-start.7
  60.5 0.6 copy-start.10
  61.1 0.6 copy-start.11

commit v2 on v1

--- a/solution.py
+++ b/solution.py
@@ -40,22 +40,32 @@
 
 
 def mixer_kernel(
-    tp, dp, tokens, lengths, norm_gain, w_gate, w_value, w_write, w_read, w_step,
-    step_bias, decay_rate, skip_gain, tap_value, tap_write, tap_read, group_gain,
-    w_out, state, hist_value, hist_write, hist_read,
-    mixed, aux, fresh,
+    tp, dp, *refs,
+):
+    count = 20
+    held_in = refs[:count]
+    mixed_out, aux_out, fresh_out = refs[count:count + 3]
+    local = refs[count + 3:2 * count + 3]
+    (
+        tokens, lengths, norm_gain, w_gate, w_value, w_write, w_read, w_step, step_bias,
+        decay_rate, skip_gain, tap_value, tap_write, tap_read, group_gain, w_out, st,
+        hist_value, hist_write, hist_read,
+    ) = local
+    (
+    mixed, aux, fresh, in_sem, out_sem,
     tok_buf, wr_send, wr_buf, conv_send, conv_buf, gain_send, gain_buf, out_buf,
-    local_w, cur, rs_send, rs_buf, mix_send, mix_buf, last_buf, st, stb,
-    tp_send, tp_recv, rs_ssem, rs_rsem, mix_ssem, mix_rsem, last_ssem, last_rsem, st_sem,
-):
+    local_w, cur, rs_send, rs_buf, mix_send, mix_buf, last_buf, stb,
+    tp_send, tp_recv, rs_ssem, rs_rsem, mix_ssem, mix_rsem, last_ssem, last_rsem,
+    ) = refs[2 * count + 3:]
+    loads = [pltpu.make_async_copy(a, b, in_sem.at[i]) for i, (a, b) in enumerate(zip(held_in, local))]
     t = lax.axis_index("tp")
     d = lax.axis_index("dp")
     rows = tokens.shape[0]
     hist_len, seq, vcols = hist_value.shape[1:]
     wcols = w_write.shape[1]
     cj = wcols // GROUPS
-    nstate = state.shape[-1]
-    hdim = state.shape[-2]
+    nstate = st.shape[-1]
+    hdim = st.shape[-2]
     feats = tokens.shape[1]
     total = feats * dp
     seqs = seq * dp
@@ -71,15 +81,19 @@
         pl.semaphore_signal(barrier, inc=1, device_id={"tp": lax.rem(t + i, tp), "dp": d}, device_id_type=MESH)
     for i in range(1, dp):
         pl.semaphore_signal(barrier, inc=1, device_id={"tp": t, "dp": lax.rem(d + i, dp)}, device_id_type=MESH)
-    st_copy = pltpu.make_async_copy(state, st, st_sem)
-    st_copy.start()
+    early = (0, 5, 6)
+    middle = (1, 11, 12, 13, 14, 17, 18, 19, 15)
+    late = tuple(i for i in range(count) if i not in early + middle and i != 16)
+    for i in early + middle + late + (16,):
+        loads[i].start()
+    for i in early:
+        loads[i].wait()
 
     size = 2 * wcols
     r, c = iota((size, size), 0), iota((size, size), 1)
     source = ((r // cj) % 2) * wcols + (r % cj) * GROUPS + r // (2 * cj)
     pick = (c == source).astype(F32)
     pick16 = pick.astype(BF16)
-    live = live_columns(lengths[...], seq, hist_len)
     for l in range(2):
         both = jnp.concatenate([w_write[l], w_read[l]], axis=0)
         got = dot(pick16, both).astype(BF16)
@@ -106,6 +120,10 @@
     got_tok = spread(TOK, lambda to: tokens, tok_buf.at[t])
     got_wr = [spread(WR0, lambda to: wr_send.at[0, to // per_group], wr_buf.at[0, :, t]), None]
 
+    for i in middle:
+        loads[i].wait()
+    got_out = [spread(OUT0, lambda to: w_out.at[0], out_buf.at[0, t]), None]
+    live = live_columns(lengths[...], seq, hist_len)
     pieces = []
     for l in range(2):
         parts = []
@@ -125,10 +143,11 @@
     gain_send[...] = jnp.concatenate([jnp.concatenate([gg, gg], axis=1), jnp.zeros((6, LANES), F32)], axis=0)
     got_conv = spread(CONV, lambda to: conv_send.at[to // per_group], conv_buf.at[:, t])
     got_gain = spread(GAIN, lambda to: gain_send, gain_buf.at[t])
-    got_out = [spread(OUT0, lambda to: w_out.at[0], out_buf.at[0, t]), None]
     got_wr[1] = spread(WR1, lambda to: wr_send.at[1, to // per_group], wr_buf.at[1, :, t])
     got_out[1] = spread(OUT1, lambda to: w_out.at[1], out_buf.at[1, t])
 
+    for i in late:
+        loads[i].wait()
     tok_buf[t] = tokens[...]
     conv_buf[:, t] = conv_send[group]
     gain_buf[t] = gain_send[...]
@@ -138,7 +157,7 @@
         local_w[l, 0] = jnp.concatenate([w_value[l], w_gate[l]], axis=0)
         local_w[l, 1] = jnp.concatenate(
             [w_write[l], w_read[l], w_step[l:l + 1], jnp.zeros((LANES - size - 1, feats), BF16)], axis=0)
-    st_copy.wait()
+    loads[16].wait()
     for l in range(2):
         stb[l] = st[l].reshape(seq * hdim, nstate).astype(BF16)
 
@@ -167,6 +186,7 @@
                 done.append((x * scale * gain).astype(BF16))
         return jnp.concatenate(done, axis=1)
 
+    stores = []
     for l in range(2):
         value = cur[...]
         x = (value * norm_gain[l:l + 1]).astype(BF16)
@@ -216,9 +236,9 @@
         write, read = acts
         u = sigmoid_mul(value_hist + tap_value[l, hist_len:hist_len + 1] * zr[:, 0:vcols])
         gate = zr[:, vcols:2 * vcols]
-        pre = step_raw + step_bias[0, l]
+        pre = step_raw + step_bias[:, l:l + 1]
         step = jnp.maximum(pre, 0.0) + jnp.log1p(jnp.exp(-jnp.abs(pre)))
-        keep = jnp.exp(-decay_rate[0, l] * step)
+        keep = jnp.exp(-decay_rate[:, l:l + 1] * step)
         read16 = read.astype(BF16)
         held = jnp.zeros((seq, 2 * hdim), F32)
         which = iota((seq, 1), 0)
@@ -228,10 +248,12 @@
         held = jnp.where(which % 2 == 0, held[:, :hdim], held[:, hdim:])
         su = step * u
         overlap = jnp.sum(write * read, axis=1, keepdims=True)
-        readout = keep * held + su * overlap + skip_gain[0, l] * u
+        readout = keep * held + su * overlap + skip_gain[:, l:l + 1] * u
         gated = readout * sigmoid_mul(gate)
         aux[l, :, 0:nstate] = write
         aux[l, :, nstate:] = jnp.concatenate([su, jnp.broadcast_to(keep, (seq, hdim))], axis=1)
+        stores.append(pltpu.make_async_copy(aux.at[l], aux_out.at[l], out_sem.at[2 * l]))
+        stores.append(pltpu.make_async_copy(fresh.at[l], fresh_out.at[l], out_sem.at[2 * l + 1]))
         mix_send[l] = jnp.concatenate([gated[:packed], gated[seq - packed:]], axis=1).astype(BF16)
         if l == 0:
             got = []
@@ -269,6 +291,8 @@
                 pl.when(to != t)(copy.start)
             else:
                 copy.start()
+    for copy in stores:
+        copy.start()
     for copy in got_out[1]:
         copy.wait_recv()
 
@@ -292,6 +316,8 @@
     for m in range(1, k_blocks):
         mine = jnp.where(t % k_blocks == m, full[m * rows:(m + 1) * rows], mine)
     mixed[...] = mine
+    stores.append(pltpu.make_async_copy(mixed, mixed_out, out_sem.at[4]))
+    stores[-1].start()
 
     for copy in sent:
         copy.wait_send()
@@ -302,6 +328,8 @@
                 pl.when(to != t)(copy.wait_send)
             else:
                 copy.wait_send()
+    for copy in stores:
+        copy.wait()
 
 
 def finish_kernel(lengths, mixed_in, aux, fresh, state, hist_value, hist_write, hist_read,
@@ -310,21 +338,25 @@
     wcols = hist_write.shape[-1]
     nstate = state.shape[-1]
     hdim = state.shape[-2]
-    l = pl.program_id(0)
-    live = live_columns(lengths[...], seq, hist_len)
-    mixed[...] = mixed_in[...]
-    edges = (
-        (hist_value, new_value, 0, vcols),
-        (hist_write, new_write, LANES, wcols),
-        (hist_read, new_read, LANES + wcols, wcols),
-    )
-    for old, new, at, width in edges:
-        for k in range(1, hist_len):
-            new[0, k - 1] = (old[0, k].astype(F32) * live[k]).astype(BF16)
-        new[0, hist_len - 1] = fresh[0, :, at:at + width]
+    first = pl.program_id(1) == 0
+
+    @pl.when(first)
+    def _():
+        live = live_columns(lengths[...], seq, hist_len)
+        mixed[...] = mixed_in[...]
+        edges = (
+            (hist_value, new_value, 0, vcols),
+            (hist_write, new_write, LANES, wcols),
+            (hist_read, new_read, LANES + wcols, wcols),
+        )
+        for old, new, at, width in edges:
+            for k in range(1, hist_len):
+                new[0, k - 1] = (old[0, k].astype(F32) * live[k]).astype(BF16)
+            new[0, hist_len - 1] = fresh[0, :, at:at + width]
+
     write = aux[0, :, 0:nstate]
     rest = aux[0, :, nstate:].T
-    for s in range(seq):
+    for s in range(state.shape[1]):
         su = rest[0:hdim, s:s + 1]
         keep = rest[hdim:, s:s + 1]
         new_state[0, s] = keep * state[0, s] + su * write[s:s + 1]
@@ -340,24 +372,32 @@
     vcols, wcols = w_value.shape[2], w_write.shape[2]
     cj = wcols // GROUPS
     packed = 16
+    chunk = 8
     lens = lengths.reshape(1, seq)
     flip = functools.partial(jnp.swapaxes, axis1=1, axis2=2)
     state4 = state.reshape(2, seq, hdim, nstate)
     hists = [flip(h) for h in (hist_value, hist_write, hist_read)]
-    vspec = pl.BlockSpec(memory_space=VMEM)
-    sspec = pl.BlockSpec(memory_space=pltpu.SMEM)
     aspec = pl.BlockSpec(memory_space=pl.ANY)
     dma = pltpu.SemaphoreType.DMA
+    operands = (
+        tokens, lens, norm_gain, flip(w_gate), flip(w_value), flip(w_write), flip(w_read),
+        jnp.transpose(w_step, (2, 0, 1)).reshape(2, feats), step_bias.T, decay_rate.T, skip_gain.T,
+        conv_value_w, conv_write_w, conv_read_w, group_gain, w_out, state4, *hists)
+    results = (
+        jax.ShapeDtypeStruct((rows, feats), F32),
+        jax.ShapeDtypeStruct((2, seq, nstate + 2 * hdim), F32),
+        jax.ShapeDtypeStruct((2, seq, 2 * LANES), BF16),
+    )
     mixed, aux, fresh = pl.pallas_call(
         functools.partial(mixer_kernel, tp, dp),
-        out_shape=(
-            jax.ShapeDtypeStruct((rows, feats), F32),
-            jax.ShapeDtypeStruct((2, seq, nstate + 2 * hdim), F32),
-            jax.ShapeDtypeStruct((2, seq, 2 * LANES), BF16),
-        ),
-        in_specs=[vspec] * 8 + [sspec] * 3 + [vspec] * 5 + [aspec] + [vspec] * 3,
-        out_specs=(vspec,) * 3,
+        out_shape=results,
+        in_specs=[aspec] * len(operands),
+        out_specs=(aspec,) * 3,
         scratch_shapes=[
+            *[VMEM(x.shape, x.dtype) for x in operands],
+            *[VMEM(x.shape, x.dtype) for x in results],
+            dma((len(operands),)),
+            dma((5,)),
             VMEM((tp, rows, feats), BF16),
             VMEM((2, GROUPS, 2, cj, feats), BF16),
             VMEM((2, 2, tp, cj, feats), BF16),
@@ -373,7 +413,6 @@
             VMEM((2, packed, LANES), BF16),
             VMEM((dp, tp, packed, LANES), BF16),
             VMEM((tp, packed, LANES), BF16),
-            VMEM((2, seq, hdim, nstate), F32),
             VMEM((2, seq * hdim, nstate), BF16),
             dma((7, tp - 1)),
             dma((7, tp - 1)),
@@ -383,32 +422,32 @@
             dma((tp * dp - 1,)),
             dma((tp,)),
             dma((tp,)),
-            dma,
         ],
         compiler_params=pltpu.CompilerParams(
-            collective_id=0, has_side_effects=True, vmem_limit_bytes=40 * 1024 * 1024),
+            collective_id=0, has_side_effects=True),
         name="mixer_blocks",
-    )(tokens, lens, norm_gain, flip(w_gate), flip(w_value), flip(w_write), flip(w_read),
-      jnp.transpose(w_step, (2, 0, 1)).reshape(2, feats), step_bias.T, decay_rate.T, skip_gain.T,
-      conv_value_w, conv_write_w, conv_read_w, group_gain, w_out, state4, *hists)
+    )(*operands)
 
     def whole(shape):
-        return pl.BlockSpec(shape, lambda l: (0,) * len(shape))
+        return pl.BlockSpec(shape, lambda l, c: (0,) * len(shape))
 
     def layer(shape):
-        return pl.BlockSpec((1,) + shape[1:], lambda l: (l,) + (0,) * (len(shape) - 1))
+        return pl.BlockSpec((1,) + shape[1:], lambda l, c: (l,) + (0,) * (len(shape) - 1))
+
+    def part(shape):
+        return pl.BlockSpec((1, chunk) + shape[2:], lambda l, c: (l, c) + (0,) * (len(shape) - 2))
 
     mixed, new_state, *fresh_hists = pl.pallas_call(
         finish_kernel,
-        grid=(2,),
+        grid=(2, seq // chunk),
         out_shape=(
             jax.ShapeDtypeStruct(mixed.shape, F32),
             jax.ShapeDtypeStruct(state4.shape, F32),
             *[jax.ShapeDtypeStruct(h.shape, BF16) for h in hists],
         ),
-        in_specs=[whole(lens.shape), whole(mixed.shape), layer(aux.shape), layer(fresh.shape),
-                  layer(state4.shape), *[layer(h.shape) for h in hists]],
-        out_specs=(whole(mixed.shape), layer(state4.shape), *[layer(h.shape) for h in hists]),
+        in_specs=[whole(lens.shape), whole(mixed.shape), part(aux.shape), layer(fresh.shape),
+                  part(state4.shape), *[layer(h.shape) for h in hists]],
+        out_specs=(whole(mixed.shape), part(state4.shape), *[layer(h.shape) for h in hists]),
         name="new_states",
     )(lens, mixed, aux, fresh, state4, *hists)
     return (mixed, new_state.reshape(state.shape), *[flip(h) for h in fresh_hists])

time: 65.9 us -> 50.4 us (0.76)
  local copies, waits for them, and re-layouts: 17 us -> 0 us
  Pallas kernels: 47.4 us -> 49.5 us
    unnamed x46 -> x0, local copies, waits for them, and re-layouts: 17 us -> none
    pallas_call x2, Pallas kernels: 47.4 us -> 49.5 us  [the longest x1 43.8 us: body(): pl.pallas_call(functools.partial(mixer_kernel, tp, dp), out_shape=results...]
where the time goes in v2:
time: 50.4 us; the launch traced here: 50.1 us
  Pallas kernels  49.5 us (98%)
  between operations  0.65 us (1%)
    pallas_call x1, Pallas kernels, body(): pl.pallas_call(functools.partial(mixer_kernel, tp, dp), out_shape=results...  43.8 us
    pallas_call x1, Pallas kernels, body(): pl.pallas_call(finish_kernel, grid=(2, seq // chunk), out_shape=(jax.Shap...  5.71 us

profile of v2, /device:TPU:0, one launch (start us, length us, event | category | flops | bytes accessed | tf_op | source)
XLA Modules:
  0.0 50.1 jit_solution(5629043766095284545)
XLA Ops:
  0.6 43.8 %mixer_blocks.1 = (f32[12,256]{1,0:T(8,128)}, f32[2,24,256]{2,1,0:T(8,128)}, bf16[2,24,256]{2,1,0:T(8,128)(2,1)}) custom-call(bf16[12,256]{1,0:T(8,128)(2,1)} %refs_0_.1, s32[1,24]{1,0:T(1,128)} %bitcast.31, f32[2,256]{1,0:T(2,128)} %refs_2_.1, bf16[2,64,256]{2,1,0:T(8,128)(2,1)} %bitcast.27, bf16[2,64,256]{2,1,0:T(8,128)(2,1)} %bitcast.28, ...), custom_call_target="tpu_custom_call" | custom-call | tf_op jit(solution)/shard_map/mixer_blocks/pallas_call | solution.py:391
  44.4 5.7 %new_states.1 = (f32[12,256]{1,0:T(8,128)}, f32[2,24,64,128]{3,2,1,0:T(8,128)}, bf16[2,3,24,64]{3,2,1,0:T(8,128)(2,1)}, bf16[2,3,24,32]{3,2,1,0:T(8,128)(2,1)}, bf16[2,3,24,32]{3,2,1,0:T(8,128)(2,1)}) custom-call(s32[1,24]{1,0:T(1,128)} %bitcast.32, f32[12,256]{1,0:T(8,128)} %get-tuple-element.13.mixed_in, f32[2,24,256]{2,1,0:T(8,128)} %get-tuple-element.14.aux, ...), custom_call_target="tpu_custom_call" | custom-call | tf_op jit(solution)/shard_map/new_states/pallas_call | solution.py:440

commit v3 on v2

--- a/solution.py
+++ b/solution.py
@@ -118,11 +118,50 @@
         return out
 
     got_tok = spread(TOK, lambda to: tokens, tok_buf.at[t])
-    got_wr = [spread(WR0, lambda to: wr_send.at[0, to // per_group], wr_buf.at[0, :, t]), None]
+    got_wr = [spread(WR0, lambda to: wr_send.at[0, to // per_group], wr_buf.at[0, :, t]), []]
+    got_out = [[], []]
+
+    def flipped(index, bit):
+        return index + bit * (1 - 2 * ((index // bit) % 2))
+
+    def hop(cat, n):
+        bit = tp >> (n + 1)
+        to = flipped(t, bit)
+        held = [t]
+        for m in range(n):
+            held = held + [flipped(h, tp >> (m + 1)) for h in held]
+        out = []
+        for i, h in enumerate(held):
+            if cat == WR1:
+                src = wr_send.at[1, 1 - group] if n == 0 else wr_buf.at[1, :, h]
+                dst = wr_buf.at[1, :, h]
+            else:
+                src = dst = out_buf.at[0 if cat == OUT0 else 1, h]
+            copy = pltpu.make_async_remote_copy(
+                src_ref=src, dst_ref=dst, send_sem=tp_send.at[cat, (1 << n) - 1 + i],
+                recv_sem=tp_recv.at[cat, (1 << n) - 1 + i], device_id={"tp": to, "dp": d}, device_id_type=MESH)
+            copy.start()
+            out.append(copy)
+        sent.extend(out)
+        return out
+
+    rounds = tp.bit_length() - 1
+
+    def middle_hops(cat, got):
+        for n in range(1, rounds - 1):
+            for copy in got:
+                copy.wait_recv()
+            got = hop(cat, n)
+        return got
+
+    def last_hop(cat, got):
+        for copy in got:
+            copy.wait_recv()
+        return hop(cat, rounds - 1)
+
 
     for i in middle:
         loads[i].wait()
-    got_out = [spread(OUT0, lambda to: w_out.at[0], out_buf.at[0, t]), None]
     live = live_columns(lengths[...], seq, hist_len)
     pieces = []
     for l in range(2):
@@ -138,13 +177,11 @@
     for g in range(GROUPS):
         for kind in range(2):
             at = (g * 2 + kind) * cj
-            conv_send[g, kind] = moved[at:at + cj]
+            conv_send[g, kind] = moved[at:at + cj].astype(BF16)
     gg = group_gain[...]
-    gain_send[...] = jnp.concatenate([jnp.concatenate([gg, gg], axis=1), jnp.zeros((6, LANES), F32)], axis=0)
+    gain_send[...] = jnp.concatenate([gg, gg], axis=1)
     got_conv = spread(CONV, lambda to: conv_send.at[to // per_group], conv_buf.at[:, t])
     got_gain = spread(GAIN, lambda to: gain_send, gain_buf.at[t])
-    got_wr[1] = spread(WR1, lambda to: wr_send.at[1, to // per_group], wr_buf.at[1, :, t])
-    got_out[1] = spread(OUT1, lambda to: w_out.at[1], out_buf.at[1, t])
 
     for i in late:
         loads[i].wait()
@@ -212,15 +249,21 @@
             copy.start()
             got.append(copy)
         sent.extend(got)
+        if l == 0:
+            bulk = {cat: hop(cat, 0) for cat in (WR1, OUT0, OUT1)}
+        else:
+            got_out[1] = last_hop(OUT1, bulk[OUT1])
         rs_buf[l, d] = rs_send[l, d]
         value_hist = sum(
             hist_value[l, k].astype(F32) * live[k] * tap_value[l, k:k + 1] for k in range(hist_len))
         if l == 0:
             for copy in got_conv + got_gain:
                 copy.wait_recv()
-            convs = [conv_buf[kind].reshape(nstate, LANES).T for kind in range(2)]
+            convs = [conv_buf[kind].reshape(nstate, LANES).astype(F32).T for kind in range(2)]
         for copy in got:
             copy.wait_recv()
+        if l == 0:
+            bulk = {cat: middle_hops(cat, bulk[cat]) for cat in (WR1, OUT0, OUT1)}
         z = sum(rs_buf[l, j].astype(F32) for j in range(dp))
         z = z * lax.rsqrt(z[:, 3 * LANES + size + 1:3 * LANES + size + 2] / total + norm_eps)
         step_raw = z[:, 3 * LANES + size:3 * LANES + size + 1]
@@ -269,6 +312,8 @@
                     got.append(copy)
             sent.extend(got)
             mix_buf[d, t] = mix_send[0]
+            got_out[0] = last_hop(OUT0, bulk[OUT0])
+            got_wr[1] = last_hop(WR1, bulk[WR1])
             for copy in got_out[0]:
                 copy.wait_recv()
             for copy in got:
@@ -332,34 +377,61 @@
         copy.wait()
 
 
-def finish_kernel(lengths, mixed_in, aux, fresh, state, hist_value, hist_write, hist_read,
-                  mixed, new_state, new_value, new_write, new_read):
+def finish_kernel(chunk, *refs):
+    ins, outs, held, made = refs[:8], refs[8:13], refs[13:21], refs[21:26]
+    in_sem, st_sem, out_sem, new_sem = refs[26:]
+    lengths, mixed_in, aux, fresh, state, hist_value, hist_write, hist_read = held
+    mixed, new_state, new_value, new_write, new_read = made
     hist_len, seq, vcols = hist_value.shape[1:]
     wcols = hist_write.shape[-1]
     nstate = state.shape[-1]
     hdim = state.shape[-2]
-    first = pl.program_id(1) == 0
-
-    @pl.when(first)
-    def _():
-        live = live_columns(lengths[...], seq, hist_len)
-        mixed[...] = mixed_in[...]
-        edges = (
-            (hist_value, new_value, 0, vcols),
-            (hist_write, new_write, LANES, wcols),
-            (hist_read, new_read, LANES + wcols, wcols),
-        )
-        for old, new, at, width in edges:
-            for k in range(1, hist_len):
-                new[0, k - 1] = (old[0, k].astype(F32) * live[k]).astype(BF16)
-            new[0, hist_len - 1] = fresh[0, :, at:at + width]
-
-    write = aux[0, :, 0:nstate]
-    rest = aux[0, :, nstate:].T
-    for s in range(state.shape[1]):
-        su = rest[0:hdim, s:s + 1]
-        keep = rest[hdim:, s:s + 1]
-        new_state[0, s] = keep * state[0, s] + su * write[s:s + 1]
+    places = [(l, at) for l in range(2) for at in range(0, seq, chunk)]
+    small = [i for i in range(8) if i != 4]
+    loads = {i: pltpu.make_async_copy(ins[i], held[i], in_sem.at[i]) for i in small}
+    blocks = []
+    stores = []
+    loads[2].start()
+    for n, (l, at) in enumerate(places):
+        blocks.append(pltpu.make_async_copy(
+            ins[4].at[l, at:at + chunk], state.at[l, at:at + chunk], st_sem.at[n]))
+        blocks[-1].start()
+    for i in small:
+        if i != 2:
+            loads[i].start()
+    loads[2].wait()
+    for n, (l, at) in enumerate(places):
+        write = aux[l, at:at + chunk, 0:nstate]
+        rest = aux[l, at:at + chunk, nstate:].T
+        blocks[n].wait()
+        for s in range(chunk):
+            su = rest[0:hdim, s:s + 1]
+            keep = rest[hdim:, s:s + 1]
+            new_state[l, at + s] = keep * state[l, at + s] + su * write[s:s + 1]
+        stores.append(pltpu.make_async_copy(
+            new_state.at[l, at:at + chunk], outs[1].at[l, at:at + chunk], new_sem.at[n]))
+        stores[-1].start()
+        if n == 0:
+            for i in small:
+                if i != 2:
+                    loads[i].wait()
+            live = live_columns(lengths[...], seq, hist_len)
+            mixed[...] = mixed_in[...]
+            edges = (
+                (hist_value, new_value, 0, vcols),
+                (hist_write, new_write, LANES, wcols),
+                (hist_read, new_read, LANES + wcols, wcols),
+            )
+            for old, new, edge, width in edges:
+                for m in range(2):
+                    for k in range(1, hist_len):
+                        new[m, k - 1] = (old[m, k].astype(F32) * live[k]).astype(BF16)
+                    new[m, hist_len - 1] = fresh[m, :, edge:edge + width]
+            for i in (0, 2, 3, 4):
+                stores.append(pltpu.make_async_copy(made[i], outs[i], out_sem.at[i]))
+                stores[-1].start()
+    for copy in stores:
+        copy.wait()
 
 
 def body(tp, dp, tokens, lengths, norm_gain, w_gate, w_value, w_write, w_read, w_step, step_bias,
@@ -401,10 +473,10 @@
             VMEM((tp, rows, feats), BF16),
             VMEM((2, GROUPS, 2, cj, feats), BF16),
             VMEM((2, 2, tp, cj, feats), BF16),
-            VMEM((GROUPS, 2, cj, LANES), F32),
-            VMEM((2, tp, cj, LANES), F32),
-            VMEM((8, LANES), F32),
-            VMEM((tp, 8, LANES), F32),
+            VMEM((GROUPS, 2, cj, LANES), BF16),
+            VMEM((2, tp, cj, LANES), BF16),
+            VMEM((2, LANES), F32),
+            VMEM((tp, 2, LANES), F32),
             VMEM((2, tp, vcols, feats), BF16),
             VMEM((2, 2, LANES, feats), BF16),
             VMEM((seq * dp, feats), F32),
@@ -428,28 +500,27 @@
         name="mixer_blocks",
     )(*operands)
 
-    def whole(shape):
-        return pl.BlockSpec(shape, lambda l, c: (0,) * len(shape))
-
-    def layer(shape):
-        return pl.BlockSpec((1,) + shape[1:], lambda l, c: (l,) + (0,) * (len(shape) - 1))
-
-    def part(shape):
-        return pl.BlockSpec((1, chunk) + shape[2:], lambda l, c: (l, c) + (0,) * (len(shape) - 2))
-
+    given = (lens, mixed, aux, fresh, state4, *hists)
+    final = (
+        jax.ShapeDtypeStruct(mixed.shape, F32),
+        jax.ShapeDtypeStruct(state4.shape, F32),
+        *[jax.ShapeDtypeStruct(h.shape, BF16) for h in hists],
+    )
+    pieces = 2 * (seq // chunk)
     mixed, new_state, *fresh_hists = pl.pallas_call(
-        finish_kernel,
-        grid=(2, seq // chunk),
-        out_shape=(
-            jax.ShapeDtypeStruct(mixed.shape, F32),
-            jax.ShapeDtypeStruct(state4.shape, F32),
-            *[jax.ShapeDtypeStruct(h.shape, BF16) for h in hists],
-        ),
-        in_specs=[whole(lens.shape), whole(mixed.shape), part(aux.shape), layer(fresh.shape),
-                  part(state4.shape), *[layer(h.shape) for h in hists]],
-        out_specs=(whole(mixed.shape), part(state4.shape), *[layer(h.shape) for h in hists]),
+        functools.partial(finish_kernel, chunk),
+        out_shape=final,
+        in_specs=[aspec] * len(given),
+        out_specs=(aspec,) * len(final),
+        scratch_shapes=[
+            *[VMEM(x.shape, x.dtype) for x in given + final],
+            dma((len(given),)),
+            dma((pieces,)),
+            dma((len(final),)),
+            dma((pieces,)),
+        ],
         name="new_states",
-    )(lens, mixed, aux, fresh, state4, *hists)
+    )(*given)
     return (mixed, new_state.reshape(state.shape), *[flip(h) for h in fresh_hists])
 
 

time: 50.4 us -> 42.8 us (0.85)
  Pallas kernels: 49.5 us -> 41.9 us
    pallas_call x1, Pallas kernels: 43.8 us -> 38.2 us  [body(): pl.pallas_call(functools.partial(mixer_kernel, tp, dp), out_shape=results...]
    pallas_call x1, Pallas kernels: 5.71 us -> 3.74 us  [body(): pl.pallas_call(functools.partial(finish_kernel, chunk), out_shape=final,...]
where the time goes in v3:
time: 42.8 us; the launch traced here: 42.6 us
  Pallas kernels  41.9 us (98%)
  between operations  0.65 us (2%)
    pallas_call x1, Pallas kernels, body(): pl.pallas_call(functools.partial(mixer_kernel, tp, dp), out_shape=results...  38.2 us
    pallas_call x1, Pallas kernels, body(): pl.pallas_call(functools.partial(finish_kernel, chunk), out_shape=final,...  3.74 us

profile of v3, /device:TPU:0, one launch (start us, length us, event | category | flops | bytes accessed | tf_op | source)
XLA Modules:
  0.0 42.6 jit_solution(10284591087516770998)
XLA Ops:
  0.6 38.2 %mixer_blocks.1 = (f32[12,256]{1,0:T(8,128)}, f32[2,24,256]{2,1,0:T(8,128)}, bf16[2,24,256]{2,1,0:T(8,128)(2,1)}) custom-call(bf16[12,256]{1,0:T(8,128)(2,1)} %refs_0_.1, s32[1,24]{1,0:T(1,128)} %bitcast.31, f32[2,256]{1,0:T(2,128)} %refs_2_.1, bf16[2,64,256]{2,1,0:T(8,128)(2,1)} %bitcast.27, bf16[2,64,256]{2,1,0:T(8,128)(2,1)} %bitcast.28, ...), custom_call_target="tpu_custom_call" | custom-call | tf_op jit(solution)/shard_map/mixer_blocks/pallas_call | solution.py:463
  38.9 3.7 %new_states.1 = (f32[12,256]{1,0:T(8,128)}, f32[2,24,64,128]{3,2,1,0:T(8,128)}, bf16[2,3,24,64]{3,2,1,0:T(8,128)(2,1)}, bf16[2,3,24,32]{3,2,1,0:T(8,128)(2,1)}, bf16[2,3,24,32]{3,2,1,0:T(8,128)(2,1)}) custom-call(s32[1,24]{1,0:T(1,128)} %bitcast.32, f32[12,256]{1,0:T(8,128)} %get-tuple-element.13.refs_1_, f32[2,24,256]{2,1,0:T(8,128)} %get-tuple-element.14.refs_2_, ...), custom_call_target="tpu_custom_call" | custom-call | tf_op jit(solution)/shard_map/new_states/pallas_call | solution.py:510

commit v4 on v3

--- a/solution.py
+++ b/solution.py
@@ -136,7 +136,9 @@
                 src = wr_send.at[1, 1 - group] if n == 0 else wr_buf.at[1, :, h]
                 dst = wr_buf.at[1, :, h]
             else:
-                src = dst = out_buf.at[0 if cat == OUT0 else 1, h]
+                layer = 0 if cat == OUT0 else 1
+                dst = out_buf.at[layer, h]
+                src = w_out.at[layer] if n == 0 else dst
             copy = pltpu.make_async_remote_copy(
                 src_ref=src, dst_ref=dst, send_sem=tp_send.at[cat, (1 << n) - 1 + i],
                 recv_sem=tp_recv.at[cat, (1 << n) - 1 + i], device_id={"tp": to, "dp": d}, device_id_type=MESH)
@@ -183,6 +185,7 @@
     got_conv = spread(CONV, lambda to: conv_send.at[to // per_group], conv_buf.at[:, t])
     got_gain = spread(GAIN, lambda to: gain_send, gain_buf.at[t])
 
+    bulk = {OUT0: hop(OUT0, 0)}
     for i in late:
         loads[i].wait()
     tok_buf[t] = tokens[...]
@@ -250,7 +253,9 @@
             got.append(copy)
         sent.extend(got)
         if l == 0:
-            bulk = {cat: hop(cat, 0) for cat in (WR1, OUT0, OUT1)}
+            bulk[OUT0] = middle_hops(OUT0, bulk[OUT0])
+            bulk[WR1] = hop(WR1, 0)
+            bulk[OUT1] = hop(OUT1, 0)
         else:
             got_out[1] = last_hop(OUT1, bulk[OUT1])
         rs_buf[l, d] = rs_send[l, d]
@@ -259,11 +264,12 @@
         if l == 0:
             for copy in got_conv + got_gain:
                 copy.wait_recv()
+            got_out[0] = last_hop(OUT0, bulk[OUT0])
             convs = [conv_buf[kind].reshape(nstate, LANES).astype(F32).T for kind in range(2)]
         for copy in got:
             copy.wait_recv()
         if l == 0:
-            bulk = {cat: middle_hops(cat, bulk[cat]) for cat in (WR1, OUT0, OUT1)}
+            bulk[WR1] = middle_hops(WR1, bulk[WR1])
         z = sum(rs_buf[l, j].astype(F32) for j in range(dp))
         z = z * lax.rsqrt(z[:, 3 * LANES + size + 1:3 * LANES + size + 2] / total + norm_eps)
         step_raw = z[:, 3 * LANES + size:3 * LANES + size + 1]
@@ -312,8 +318,8 @@
                     got.append(copy)
             sent.extend(got)
             mix_buf[d, t] = mix_send[0]
-            got_out[0] = last_hop(OUT0, bulk[OUT0])
             got_wr[1] = last_hop(WR1, bulk[WR1])
+            bulk[OUT1] = middle_hops(OUT1, bulk[OUT1])
             for copy in got_out[0]:
                 copy.wait_recv()
             for copy in got:

time: 42.8 us -> 41.2 us (0.963)
  Pallas kernels: 41.9 us -> 40.4 us
    pallas_call x1, Pallas kernels: 38.2 us -> 36.6 us  [body(): pl.pallas_call(functools.partial(mixer_kernel, tp, dp), out_shape=results...]
where the time goes in v4:
time: 41.2 us; the launch traced here: 41 us
  Pallas kernels  40.4 us (98%)
  between operations  0.65 us (2%)
    pallas_call x1, Pallas kernels, body(): pl.pallas_call(functools.partial(mixer_kernel, tp, dp), out_shape=results...  36.6 us
    pallas_call x1, Pallas kernels, body(): pl.pallas_call(functools.partial(finish_kernel, chunk), out_shape=final,...  3.74 us

profile of v4, /device:TPU:0, one launch (start us, length us, event | category | flops | bytes accessed | tf_op | source)
XLA Modules:
  0.0 41.0 jit_solution(2218547031810669972)
XLA Ops:
  0.6 36.6 %mixer_blocks.1 = (f32[12,256]{1,0:T(8,128)}, f32[2,24,256]{2,1,0:T(8,128)}, bf16[2,24,256]{2,1,0:T(8,128)(2,1)}) custom-call(bf16[12,256]{1,0:T(8,128)(2,1)} %refs_0_.1, s32[1,24]{1,0:T(1,128)} %bitcast.31, f32[2,256]{1,0:T(2,128)} %refs_2_.1, bf16[2,64,256]{2,1,0:T(8,128)(2,1)} %bitcast.27, bf16[2,64,256]{2,1,0:T(8,128)(2,1)} %bitcast.28, ...), custom_call_target="tpu_custom_call" | custom-call | tf_op jit(solution)/shard_map/mixer_blocks/pallas_call | solution.py:469
  37.3 3.7 %new_states.1 = (f32[12,256]{1,0:T(8,128)}, f32[2,24,64,128]{3,2,1,0:T(8,128)}, bf16[2,3,24,64]{3,2,1,0:T(8,128)(2,1)}, bf16[2,3,24,32]{3,2,1,0:T(8,128)(2,1)}, bf16[2,3,24,32]{3,2,1,0:T(8,128)(2,1)}) custom-call(s32[1,24]{1,0:T(1,128)} %bitcast.32, f32[12,256]{1,0:T(8,128)} %get-tuple-element.13.refs_1_, f32[2,24,256]{2,1,0:T(8,128)} %get-tuple-element.14.refs_2_, ...), custom_call_target="tpu_custom_call" | custom-call | tf_op jit(solution)/shard_map/new_states/pallas_call | solution.py:516

commit v5 on v4

--- a/solution.py
+++ b/solution.py
@@ -253,7 +253,6 @@
             got.append(copy)
         sent.extend(got)
         if l == 0:
-            bulk[OUT0] = middle_hops(OUT0, bulk[OUT0])
             bulk[WR1] = hop(WR1, 0)
             bulk[OUT1] = hop(OUT1, 0)
         else:
@@ -264,12 +263,11 @@
         if l == 0:
             for copy in got_conv + got_gain:
                 copy.wait_recv()
-            got_out[0] = last_hop(OUT0, bulk[OUT0])
             convs = [conv_buf[kind].reshape(nstate, LANES).astype(F32).T for kind in range(2)]
         for copy in got:
             copy.wait_recv()
         if l == 0:
-            bulk[WR1] = middle_hops(WR1, bulk[WR1])
+            bulk[OUT0] = middle_hops(OUT0, bulk[OUT0])
         z = sum(rs_buf[l, j].astype(F32) for j in range(dp))
         z = z * lax.rsqrt(z[:, 3 * LANES + size + 1:3 * LANES + size + 2] / total + norm_eps)
         step_raw = z[:, 3 * LANES + size:3 * LANES + size + 1]
@@ -318,8 +316,10 @@
                     got.append(copy)
             sent.extend(got)
             mix_buf[d, t] = mix_send[0]
+            bulk[WR1] = middle_hops(WR1, bulk[WR1])
+            got_out[0] = last_hop(OUT0, bulk[OUT0])
+            bulk[OUT1] = middle_hops(OUT1, bulk[OUT1])
             got_wr[1] = last_hop(WR1, bulk[WR1])
-            bulk[OUT1] = middle_hops(OUT1, bulk[OUT1])
             for copy in got_out[0]:
                 copy.wait_recv()
             for copy in got:

time: 41.2 us -> 43.6 us (1.058)
  Pallas kernels: 40.4 us -> 42.7 us
    pallas_call x1, Pallas kernels: 36.6 us -> 39 us  [body(): pl.pallas_call(functools.partial(mixer_kernel, tp, dp), out_shape=results...]
where the time goes in v5:
time: 43.6 us; the launch traced here: 43.4 us
  Pallas kernels  42.7 us (98%)
  between operations  0.65 us (1%)
    pallas_call x1, Pallas kernels, body(): pl.pallas_call(functools.partial(mixer_kernel, tp, dp), out_shape=results...  39 us
    pallas_call x1, Pallas kernels, body(): pl.pallas_call(functools.partial(finish_kernel, chunk), out_shape=final,...  3.74 us

profile of v5, /device:TPU:0, one launch (start us, length us, event | category | flops | bytes accessed | tf_op | source)
XLA Modules:
  0.0 43.4 jit_solution(12684005174267896405)
XLA Ops:
  0.6 39.0 %mixer_blocks.1 = (f32[12,256]{1,0:T(8,128)}, f32[2,24,256]{2,1,0:T(8,128)}, bf16[2,24,256]{2,1,0:T(8,128)(2,1)}) custom-call(bf16[12,256]{1,0:T(8,128)(2,1)} %refs_0_.1, s32[1,24]{1,0:T(1,128)} %bitcast.31, f32[2,256]{1,0:T(2,128)} %refs_2_.1, bf16[2,64,256]{2,1,0:T(8,128)(2,1)} %bitcast.27, bf16[2,64,256]{2,1,0:T(8,128)(2,1)} %bitcast.28, ...), custom_call_target="tpu_custom_call" | custom-call | tf_op jit(solution)/shard_map/mixer_blocks/pallas_call | solution.py:469
  39.6 3.7 %new_states.1 = (f32[12,256]{1,0:T(8,128)}, f32[2,24,64,128]{3,2,1,0:T(8,128)}, bf16[2,3,24,64]{3,2,1,0:T(8,128)(2,1)}, bf16[2,3,24,32]{3,2,1,0:T(8,128)(2,1)}, bf16[2,3,24,32]{3,2,1,0:T(8,128)(2,1)}) custom-call(s32[1,24]{1,0:T(1,128)} %bitcast.32, f32[12,256]{1,0:T(8,128)} %get-tuple-element.13.refs_1_, f32[2,24,256]{2,1,0:T(8,128)} %get-tuple-element.14.refs_2_, ...), custom_call_target="tpu_custom_call" | custom-call | tf_op jit(solution)/shard_map/new_states/pallas_call | solution.py:516
